TPU v7x, 256 devices: a whole 4x4x8 slice. The times are simulated.
256 devices in a mesh: sp: 64 (over z, y, core), tp: 4 (over x).
Axes of the slice: x: 4, y: 4, z: 8, core: 2. Of those that a mesh axis runs over, the one named last changes fastest.
Arguments:
- cotangent: bfloat16 [16384, 2048], P('sp'), may hold values from -16 to 16
- stream_in: bfloat16 [16384, 2048], P('sp'), may hold values from -6 to 6
- norm_gain: float32 [2048], replicated, may hold values from 0.1 to 1.9
- out_gate: bfloat16 [16384, 1024], P('sp', 'tp'), may hold values from -6 to 6
- in_gate: bfloat16 [16384, 1024], P('sp', 'tp'), may hold values from -6 to 6
- conv_input: bfloat16 [16384, 1024], P('sp', 'tp'), may hold values from -6 to 6
- conv_taps: float32 [3, 1024], P(None, 'tp'), may hold values from -3 to 3
- out_weight: bfloat16 [2048, 1024], P(None, 'tp'), may hold values from -0.1875 to 0.1875
- expert_gate: bfloat16 [64, 2048, 1024], P('sp', None, 'tp'), may hold values from -0.125 to 0.125
- expert_up: bfloat16 [64, 2048, 1024], P('sp', None, 'tp'), may hold values from -0.125 to 0.125
- expert_down: bfloat16 [64, 1024, 2048], P('sp', 'tp'), may hold values from -0.1875 to 0.1875
- expert_choice: int32 [16384, 2], P('sp'), may hold values from 0 to 63, all different within a row; in each aligned block of 256 rows (0 to 255, 256 to 511, ...) at most 16 rows name the same one
- route_scale: float32 [16384, 2], P('sp'), may hold values from 0.05 to 0.6
Outputs:
- grad_stream: bfloat16 [16384, 2048], P('sp', 'tp')
- grad_out_gate: bfloat16 [16384, 1024], P('sp', 'tp')
- grad_in_gate: bfloat16 [16384, 1024], P('sp', 'tp')
- grad_conv_input: bfloat16 [16384, 1024], P('sp', 'tp')
- grad_out_weight: float32 [2048, 1024], P('sp', 'tp')
- grad_expert_gate: float32 [64, 2048, 1024], P('sp', None, 'tp')
- grad_expert_up: float32 [64, 2048, 1024], P('sp', None, 'tp')
- grad_expert_down: float32 [64, 1024, 2048], P('sp', 'tp')
Inputs may be any that keep to these rules, and one draw needn't show every extreme that they name: `expert_choice`: each row names two different experts. Within the rows of one device no expert is named more than 16 times, a bound that some block reaches in some devices' rows.
All inputs are finite; a program needn't handle non-finite values.
Results may differ from a plain program's by a relative error of at most 0.01.
Values may be sent and summed in bfloat16 or wider, within the bound.
No kernel may reach another device: no remote copies, remote signals or barrier semaphores. Data moves between devices by JAX's collectives and lax.ppermute only.
A program may use at most 128 MiB of HBM per device.

v0:
```python
import jax
import jax.numpy as jnp
from jax import lax
from jax.experimental import pallas as pl
from jax.experimental.pallas import tpu as pltpu
from jax.sharding import PartitionSpec as P


norm_eps = 1e-06
bf16 = jnp.bfloat16
f32 = jnp.float32


WHOLE = pl.BlockSpec(memory_space=pltpu.VMEM)
SCALAR = pl.BlockSpec(memory_space=pltpu.SMEM)


def call(body, outs, operands, flops=0, moved=0, limit=60 * 1024 * 1024, scalars=1):
    return pl.pallas_call(
        body,
        out_shape=[jax.ShapeDtypeStruct(shape, dtype) for shape, dtype in outs],
        in_specs=[SCALAR] * scalars + [WHOLE] * (len(operands) - scalars),
        out_specs=[WHOLE] * len(outs),
        cost_estimate=pl.CostEstimate(flops=flops, bytes_accessed=moved, transcendentals=0),
        compiler_params=pltpu.CompilerParams(vmem_limit_bytes=limit),
    )(*operands)


def dot(left, right, contract):
    return lax.dot_general(
        left, right, ((contract[:1], contract[1:]), ((), ())), preferred_element_type=f32
    )


def ring(size, steps):
    return [(k, (k + steps) % size) for k in range(size)]


def send_kernel(tp_ref, choice_ref, scale_ref, stream_ref, gain_ref, cot_ref, rms_ref, *outs):
    tokens, _ = stream_ref.shape
    chunks = len(outs) // 2
    experts, part, columns = outs[0].shape
    part = part // 2
    start = pl.multiple_of(tp_ref[0] * columns, columns)
    first_id, second_id = choice_ref[0:1, :], choice_ref[1:2, :]
    expert_iota = lax.broadcasted_iota(jnp.int32, (experts, tokens), 0)
    first, second = first_id == expert_iota, second_id == expert_iota
    named = jnp.where(first | second, 1.0, 0.0).astype(bf16)
    row = lax.broadcasted_iota(jnp.int32, (tokens, tokens), 0)
    col = lax.broadcasted_iota(jnp.int32, (tokens, tokens), 1)
    before = jnp.where(row < col, 1.0, 0.0).astype(bf16)
    earlier = dot(named, before, (1, 0))
    slots = []
    for chosen, ids in ((first, first_id), (second, second_id)):
        place = jnp.sum(jnp.where(chosen, earlier, 0.0), axis=0, keepdims=True).astype(jnp.int32)
        chunk = lax.div(place, part)
        slots.append(chunk * (experts * part) + ids * part + (place - chunk * part))
    stream = stream_ref[...].astype(f32)
    inverse_rms = lax.rsqrt(jnp.mean(stream * stream, axis=-1, keepdims=True) + norm_eps)
    rms_ref[...] = inverse_rms
    stream_cols = stream_ref[:, pl.ds(start, columns)].astype(f32)
    normed = (stream_cols * inverse_rms * gain_ref[:, pl.ds(start, columns)]).astype(bf16)
    cot = cot_ref[:, pl.ds(start, columns)]
    slot_iota = lax.broadcasted_iota(jnp.int32, (experts * part, tokens), 0)
    for c in range(chunks):
        send_ref, pick_ref = outs[2 * c : 2 * c + 2]
        here = slot_iota + c * experts * part
        pick_first, pick_second = slots[0] == here, slots[1] == here
        pick = jnp.where(pick_first | pick_second, 1.0, 0.0).astype(bf16)
        pick_ref[...] = pick
        send_ref[:, :part, :] = dot(pick, normed, (1, 0)).astype(bf16).reshape(experts, part, columns)
        scale = jnp.where(pick_first, scale_ref[0:1, :], 0.0) + jnp.where(
            pick_second, scale_ref[1:2, :], 0.0
        )
        weight = jnp.sum(scale, axis=1, keepdims=True)
        send_ref[:, part:, :] = (
            (dot(pick, cot, (1, 0)) * weight).astype(bf16).reshape(experts, part, columns)
        )


def block(ref, k, parts=2, half=None):
    part = ref.shape[1] // parts
    peers = slice(None)
    if half is not None:
        peers = pl.ds(pl.multiple_of(half * (ref.shape[0] // 2), ref.shape[0] // 2), ref.shape[0] // 2)
    return ref[peers, k * part : (k + 1) * part, :].reshape(-1, ref.shape[2])


def gathered_blocks(refs, half=None):
    own, after, before, far_rows, far_scaled = refs
    rows = [block(r, 0, p, half) for r, p in ((own, 2), (after, 2), (far_rows, 1), (before, 2))]
    scaled = [
        block(r, k, p, half)
        for r, k, p in ((own, 1, 2), (after, 1, 2), (far_scaled, 0, 1), (before, 1, 2))
    ]
    return rows, scaled


def column_starts(tp_ref, columns):
    return [pl.multiple_of(lax.rem(tp_ref[0] + j, 4) * columns, columns) for j in range(4)]


def for_each_half(rows, step):
    def one(half, carry):
        step(half, pl.ds(pl.multiple_of(half * (rows // 2), rows // 2), rows // 2))
        return carry

    lax.fori_loop(0, 2, one, 0)


def first_products(rows, scaled, gate_ref, up_ref, down_ref, starts):
    columns = rows[0].shape[1]
    gate_pre = up_pre = hidden_grad = 0.0
    for row, scaled_row, start in zip(rows, scaled, starts):
        gate_pre = gate_pre + dot(row, gate_ref[0, pl.ds(start, columns), :], (1, 0))
        up_pre = up_pre + dot(row, up_ref[0, pl.ds(start, columns), :], (1, 0))
        hidden_grad = hidden_grad + dot(scaled_row, down_ref[0, :, pl.ds(start, columns)], (1, 1))
    return gate_pre, up_pre, hidden_grad


def expert_start_kernel(tp_ref, own, after, before, gate_ref, up_ref, down_ref, *outs):
    starts = column_starts(tp_ref, own.shape[2])

    def step(half, here):
        sums = first_products(
            [block(ref, 0, 2, half) for ref in (own, after, before)],
            [block(ref, 1, 2, half) for ref in (own, after, before)],
            gate_ref, up_ref, down_ref, [starts[j] for j in (0, 1, 3)],
        )
        for ref, value in zip(outs, sums):
            ref[here, :] = value

    for_each_half(outs[0].shape[0], step)


def expert_kernel(tp_ref, *refs):
    weights, outs = refs[5:8], refs[8:]
    gate_ref, up_ref, _ = weights
    hidden_ref, ggrad_ref, ugrad_ref, *places = outs
    starts = column_starts(tp_ref, refs[0].shape[2])
    columns = refs[0].shape[2]

    def step(half, here):
        if len(refs[4].shape) == 3:
            rows, scaled = gathered_blocks(refs[:5], half)
            gate_pre, up_pre, hidden_grad = first_products(rows, scaled, *weights, starts)
        else:
            far = first_products(
                [block(refs[0], 0, 1, half)], [block(refs[1], 0, 1, half)], *weights, starts[2:3]
            )
            gate_pre, up_pre, hidden_grad = (
                ref[here, :] + value for ref, value in zip(refs[2:5], far)
            )
        sigmoid_gate = jax.nn.sigmoid(gate_pre)
        silu_gate = gate_pre * sigmoid_gate
        hidden_ref[here, :] = (silu_gate * up_pre).astype(bf16)
        gate_grad = (
            hidden_grad * up_pre * sigmoid_gate * (1.0 + gate_pre * (1.0 - sigmoid_gate))
        ).astype(bf16)
        up_grad = (hidden_grad * silu_gate).astype(bf16)
        ggrad_ref[here, :] = gate_grad
        ugrad_ref[here, :] = up_grad
        for place, start in zip(places, starts):
            place[here, :] = (
                dot(gate_grad, gate_ref[0, pl.ds(start, columns), :], (1, 1))
                + dot(up_grad, up_ref[0, pl.ds(start, columns), :], (1, 1))
            ).astype(bf16)

    for_each_half(hidden_ref.shape[0], step)


def weights_kernel(tp_ref, *refs):
    chunks = (len(refs) - 3) // 8
    outs = refs[-3:]
    columns = refs[0].shape[2]
    starts = column_starts(tp_ref, columns)
    part = refs[0].shape[1] // 2

    def step(half, here):
        for j in range(4):
            gate = up = down = 0.0
            for c in range(chunks):
                own, after, before, far_rows, far_scaled = refs[8 * c : 8 * c + 5]
                ref = (own, after, far_rows, before)[j]
                rows = ref[:, :part, here].reshape(-1, columns // 2)
                if j == 2:
                    scaled = far_scaled[:, :, here].reshape(-1, columns // 2)
                else:
                    scaled = ref[:, part:, here].reshape(-1, columns // 2)
                hidden, gate_grad, up_grad = (refs[8 * c + 5 + k][...] for k in range(3))
                gate = gate + dot(rows, gate_grad, (0, 0))
                up = up + dot(rows, up_grad, (0, 0))
                down = down + dot(hidden, scaled, (0, 0))
            cols = pl.ds(pl.multiple_of(starts[j] + half * (columns // 2), columns // 2), columns // 2)
            outs[0][0, cols, :] = gate
            outs[1][0, cols, :] = up
            outs[2][0, :, cols] = down

    for_each_half(columns, step)


def token_kernel(
    tp_ref, pick0, back0, pick1, back1, stream_ref, gain_ref, rms_ref, token_ref, sum_ref
):
    columns = token_ref.shape[1]
    start = column_starts(tp_ref, columns)[0]
    token = (
        dot(pick0[...], block(back0, 0, 1), (0, 0)) + dot(pick1[...], block(back1, 0, 1), (0, 0))
    ).astype(bf16)
    token_ref[...] = token
    unit = stream_ref[:, pl.ds(start, columns)].astype(f32) * rms_ref[...]
    unit_grad = token.astype(f32) * gain_ref[:, pl.ds(start, columns)]
    row_sum = jnp.sum(unit * unit_grad, axis=-1, keepdims=True)
    sum_ref[...] = jnp.transpose(jnp.broadcast_to(row_sum, (row_sum.shape[0], 128)))[0:1, :]


def stream_grads(token, cot, stream, gain, inverse_rms, along):
    unit = stream.astype(f32) * inverse_rms
    unit_grad = token.astype(f32) * gain
    return (cot.astype(f32) + inverse_rms * (unit_grad - unit * along)).astype(bf16)


def grad_kernel(
    tp_ref, core_ref, token_ref, s0, s1, s2, s3, stream_ref, cot_ref, gain_ref, rms_ref,
    m0, m1, m2, m3, gstream_ref, along_ref, keep_ref, give_ref,
):
    columns = token_ref.shape[1]
    start = column_starts(tp_ref, columns)[0]
    total = (s0[...] + s1[...] + s2[...] + s3[...]) * (1.0 / (4 * columns))
    along = jnp.transpose(jnp.broadcast_to(total, (128, total.shape[1])))[:, 0:1]
    along_ref[...] = along
    here = pl.ds(start, columns)
    grad = stream_grads(
        token_ref[...], cot_ref[:, here], stream_ref[:, here], gain_ref[:, here], rms_ref[...], along
    )
    gstream_ref[...] = grad
    products = [
        dot(grad, m[...], (0, 0)).astype(bf16).reshape(*keep_ref.shape[:1], *keep_ref.shape[2:])
        for m in (m0, m1, m2, m3)
    ]
    matching = lax.rem(tp_ref[0] + core_ref[0], 2) == 0
    places = [lax.rem(tp_ref[0] + j, 4) // 2 for j in range(4)]
    for j in (0, 2):
        even, odd = products[j][:, None], products[j + 1][:, None]
        even_at, odd_at = places[j], places[j + 1]
        keep_ref[:, pl.ds(jnp.where(matching, even_at, odd_at), 1)] = jnp.where(matching, even, odd)
        give_ref[:, pl.ds(jnp.where(matching, odd_at, even_at), 1)] = jnp.where(matching, odd, even)


def mixed_kernel(
    tp_ref, g0, t1, t2, t3, stream_ref, cot_ref, gain_ref, rms_ref, along_ref, weight_ref,
    filtered_ref, gate_ref, ggate_ref, fgrad_ref,
):
    columns = g0.shape[1]
    starts = column_starts(tp_ref, columns)
    mixed_grad = dot(g0[...], weight_ref[pl.ds(starts[0], columns), :], (1, 0))
    for token_ref, start in zip((t1, t2, t3), starts[1:]):
        here = pl.ds(start, columns)
        grad = stream_grads(
            token_ref[...], cot_ref[:, here], stream_ref[:, here], gain_ref[:, here], rms_ref[...],
            along_ref[...],
        )
        mixed_grad = mixed_grad + dot(grad, weight_ref[here, :], (1, 0))
    ggate_ref[...] = (mixed_grad * filtered_ref[...]).astype(bf16)
    fgrad_ref[...] = mixed_grad * gate_ref[...].astype(f32)


def shift_edge(value, axis, steps):
    count = lax.axis_size(axis)
    first, last = (max(0, -steps), min(count, count - steps))
    return lax.ppermute(value, axis, [(source, source + steps) for source in range(first, last)])


def exchange(array, axis, groups=None):
    return lax.all_to_all(
        array, axis, split_axis=0, concat_axis=0, tiled=True, axis_index_groups=groups
    )


def body(
    cotangent, stream_in, norm_gain, out_gate, in_gate, conv_input, conv_taps, out_weight,
    expert_gate, expert_up, expert_down, expert_choice, route_scale,
):
    sp_size = lax.axis_size("sp")
    tp_size = lax.axis_size("tp")
    tokens, width = stream_in.shape
    columns = width // tp_size
    capacity = 4 * tokens // sp_size
    chunks = 2
    part = capacity // chunks
    right, left = ring(tp_size, 1), ring(tp_size, -1)
    tp = lax.axis_index("tp").astype(jnp.int32).reshape(1)
    gain = norm_gain.reshape(1, width)

    sent_block = ((sp_size, 2 * part, columns), bf16)
    inverse_rms, *sent = call(
        send_kernel,
        [((tokens, 1), f32)] + [sent_block, ((sp_size * part, tokens), bf16)] * chunks,
        [tp, expert_choice.T, route_scale.T, stream_in, gain, cotangent],
    )
    picks = sent[1::2]

    def send_along(value, pairs):
        return lax.ppermute(value, "tp", pairs)

    gathered = []
    for c in range(chunks):
        own = exchange(sent[2 * c], "sp")
        before = send_along(own, right)
        after = send_along(own, left)
        far_rows = send_along(before[:, :part], right)
        far_scaled = send_along(after[:, part:], left)
        gathered.append([own, after, before, far_rows, far_scaled])

    returned = []
    saved = []
    rows_here = sp_size * part
    ff = expert_gate.shape[2]
    half = rows_here // 2
    for c in range(chunks):
        ahead = c < chunks - 1
        operands = gathered[c]
        weights = [expert_gate, expert_up, expert_down]
        if not ahead:
            started = call(
                expert_start_kernel,
                [((rows_here, ff), f32)] * 3,
                [tp, *operands[:3], *weights],
                flops=5 * rows_here * width * ff,
            )
            operands = [*operands[3:], *started]
        hidden, gate_grad, up_grad, p0, p1, p2, p3 = call(
            expert_kernel,
            [((rows_here, ff), bf16)] * 3 + [((rows_here, columns), bf16)] * 4,
            [tp, *operands, *weights],
            flops=10 * rows_here * width * ff,
        )
        saved += [*gathered[c], hidden, gate_grad, up_grad]
        if ahead:
            nothing = jnp.zeros((half, columns), bf16)
            to_next = send_along(p2[:half], right)
            to_last = send_along(p2[half:], left)
            p1 = (p1.astype(f32) + jnp.concatenate([to_next, nothing]).astype(f32)).astype(bf16)
            p3 = (p3.astype(f32) + jnp.concatenate([nothing, to_last]).astype(f32)).astype(bf16)
        from_last = send_along(p1, right)
        from_next = send_along(p3, left)
        slot_grad = p0.astype(f32) + from_last.astype(f32) + from_next.astype(f32)
        if not ahead:
            slot_grad = slot_grad + send_along(p2, ring(tp_size, 2)).astype(f32)
        slot_grad = slot_grad.astype(bf16).reshape(sp_size, part, columns)
        returned.append(exchange(slot_grad, "sp"))

    grad_gate, grad_up, grad_down = call(
        weights_kernel,
        [(expert_gate.shape, f32), (expert_up.shape, f32), (expert_down.shape, f32)],
        [tp, *saved],
        flops=6 * sp_size * capacity * width * ff,
    )

    product = in_gate.astype(f32) * conv_input.astype(f32)
    earlier = shift_edge(product[-2:], "sp", 1)
    extended = jnp.concatenate([earlier, product], axis=0)
    filtered = conv_taps[0] * product + conv_taps[1] * extended[1:-1] + conv_taps[2] * extended[:-2]
    mixed_in = (out_gate.astype(f32) * filtered).astype(bf16)

    from_peers = (left, ring(tp_size, 2), right)

    def to_peers(value):
        return [value] + [send_along(value, pairs) for pairs in from_peers]

    mixed_blocks = to_peers(mixed_in)
    token_cols, row_sum = call(
        token_kernel,
        [((tokens, columns), bf16), ((1, tokens), f32)],
        [tp, picks[0], returned[0], picks[1], returned[1], stream_in, gain, inverse_rms],
    )
    row_sums = to_peers(row_sum)
    token_blocks = to_peers(token_cols)
    core = lax.rem(lax.axis_index("sp"), 2).astype(jnp.int32).reshape(1)
    rows_out = width // sp_size
    pieces = ((columns // rows_out, tp_size // 2, rows_out, out_weight.shape[1]), bf16)
    grad_stream, along, keep, give = call(
        grad_kernel,
        [((tokens, columns), bf16), ((tokens, 1), f32), pieces, pieces],
        [
            tp, core, token_cols, *row_sums, stream_in, cotangent, gain, inverse_rms,
            *mixed_blocks,
        ],
        scalars=2,
    )
    grad_out_gate, filtered_grad = call(
        mixed_kernel,
        [(out_gate.shape, bf16), (out_gate.shape, f32)],
        [
            tp, grad_stream, *token_blocks[1:], stream_in, cotangent, gain, inverse_rms, along,
            out_weight, filtered, out_gate,
        ],
    )
    later = shift_edge(filtered_grad[:2], "sp", -1)
    extended_grad = jnp.concatenate([filtered_grad, later], axis=0)
    product_grad = (
        conv_taps[0] * filtered_grad
        + conv_taps[1] * extended_grad[1:-1]
        + conv_taps[2] * extended_grad[2:]
    )
    grad_in_gate = (product_grad * conv_input.astype(f32)).astype(bf16)
    grad_conv_input = (product_grad * in_gate.astype(f32)).astype(bf16)

    taken = lax.ppermute(give, "sp", [(k, k ^ 1) for k in range(sp_size)])
    keep = (keep.astype(f32) + taken.astype(f32)).astype(bf16)
    same_core = [[2 * k + c for k in range(sp_size // 2)] for c in range(2)]
    keep = keep.reshape(sp_size // 2, rows_out, out_weight.shape[1])
    reduced = exchange(keep, "sp", same_core).astype(f32).sum(axis=0)
    blocks = sp_size // tp_size
    placed = [
        (j * tp_size + q, (q * blocks + j // tp_size) * tp_size + j % tp_size)
        for j in range(sp_size)
        for q in range(tp_size)
    ]
    grad_out_weight = lax.ppermute(reduced, ("sp", "tp"), placed)
    return (
        grad_stream, grad_out_gate, grad_in_gate, grad_conv_input, grad_out_weight,
        grad_gate, grad_up, grad_down,
    )


def solution(mesh):
    return jax.shard_map(
        body,
        mesh=mesh,
        in_specs=(
            P("sp", None), P("sp", None), P(), P("sp", "tp"), P("sp", "tp"), P("sp", "tp"),
            P(None, "tp"), P(None, "tp"), P("sp", None, "tp"), P("sp", None, "tp"),
            P("sp", "tp", None), P("sp", None), P("sp", None),
        ),
        out_specs=(
            P("sp", "tp"), P("sp", "tp"), P("sp", "tp"), P("sp", "tp"), P("sp", "tp"),
            P("sp", None, "tp"), P("sp", None, "tp"), P("sp", "tp", None),
        ),
        check_vma=False,
    )
```

profile of v0, /device:TPU:121, one launch (start us, length us, event | category | flops | bytes accessed | tf_op | source)
XLA Modules:
  0.0 285.2 jit_solution(18025549831897267368)
XLA Ops:
  0.6 4.1 %shard_map.188 = (f32[256,1]{1,0:T(8,128)}, bf16[64,16,512]{2,1,0:T(8,128)(2,1)}, bf16[512,256]{1,0:T(8,128)(2,1)}, bf16[64,16,512]{2,1,0:T(8,128)(2,1)}, bf16[512,256]{1,0:T(8,128)(2,1)}) custom-call(s32[1]{0:T(128)} %bitcast.tp_ref, s32[2,256]{1,0:T(2,128)} %bitcast.23, f32[2,256]{1,0:T(2,128)} %bitcast.24, bf16[256,2048]{1,0:T(8,128)(2,1)} %stream_ref.7, ...), custom_call_target="tpu_custom_call" | custom-call | tf_op jit(solution)/shard_map/pallas_call | solution.py:19
  4.7 36.7 %all_to_all.25.own.refs_8_ = bf16[64,16,512]{2,1,0:T(8,128)(2,1)S(1)} all-to-all(bf16[64,16,512]{2,1,0:T(8,128)(2,1)} %get-tuple-element.48), channel_id=1, replica_groups=mesh['sp'=64,'tp'=4] {'sp'}, dimensions={0} | all-to-all | bytes 2097152 | tf_op jit(solution)/shard_map/all_to_all | solution.py:275
  41.5 8.8 %all-to-all-start = ((bf16[64,16,512]{2,1,0:T(8,128)(2,1)}), bf16[64,16,512]{2,1,0:T(8,128)(2,1)}, u32[]{:S(2)}, u32[]{:S(2)}) async-start(bf16[64,16,512]{2,1,0:T(8,128)(2,1)} %get-tuple-element.42), calls=%async_computation | async-start | bytes 2097152 | tf_op jit(solution)/shard_map/all_to_all | solution.py:275
  50.3 1.3 collective-permute-start.8
  51.5 1.5 collective-permute-start.10
  53.0 23.0 %all-to-all-done.refs_0_ = bf16[64,16,512]{2,1,0:T(8,128)(2,1)} async-done(((bf16[64,16,512]{2,1,0:T(8,128)(2,1)}), bf16[64,16,512]{2,1,0:T(8,128)(2,1)}, u32[]{:S(2)}, u32[]{:S(2)}) %all-to-all-start) | async-done | bytes 1048608 | tf_op jit(solution)/shard_map/all_to_all | solution.py:275
  76.0 1.2 collective-permute-start.1
  77.2 1.5 collective-permute-start
  79.8 2.6 collective-permute-start.11
  82.4 18.9 %collective-permute-done.1.refs_2_ = bf16[64,16,512]{2,1,0:T(8,128)(2,1)S(1)} collective-permute-done((bf16[64,16,512]{2,1,0:T(8,128)(2,1)}, bf16[64,16,512]{2,1,0:T(8,128)(2,1)S(1)}, u32[]{:S(2)}, u32[]{:S(2)}) %collective-permute-start.1) | collective-permute-done | bytes 1048608 | tf_op jit(solution)/shard_map/ppermute | solution.py:304
  103.1 1.0 copy-done.16
  104.9 2.7 collective-permute-start.3
  107.6 5.4 %shard_map.190 = (f32[512,256]{1,0:T(8,128)}, f32[512,256]{1,0:T(8,128)}, f32[512,256]{1,0:T(8,128)}) custom-call(s32[1]{0:T(128)} %bitcast.tp_ref, bf16[64,16,512]{2,1,0:T(8,128)(2,1)} %copy-done, bf16[64,16,512]{2,1,0:T(8,128)(2,1)} %copy-done.2, bf16[64,16,512]{2,1,0:T(8,128)(2,1)} %copy-done.1, bf16[1,2048,256]{2,1,0:T(8,128)(2,1)} %refs_5_.3, ...), custom_call_target="tpu_custom_call" | custom-call | flops 1342177280 | tf_op jit(solution)/shard_map/pallas_call | solution.py:19
  113.0 5.9 %shard_map.191 = (bf16[512,256]{1,0:T(8,128)(2,1)}, bf16[512,256]{1,0:T(8,128)(2,1)}, bf16[512,256]{1,0:T(8,128)(2,1)}, bf16[512,512]{1,0:T(8,128)(2,1)}, bf16[5...) custom-call(s32[1]{0:T(128)} %bitcast.tp_ref, ...), custom_call_target="tpu_custom_call" | custom-call | flops 2684354560 | tf_op jit(solution)/shard_map/pallas_call | solution.py:19
  119.0 1.7 collective-permute-start.14
  120.7 1.2 collective-permute-start.13
  122.2 1.7 collective-permute-done.2.refs_3_
  123.8 8.5 %shard_map.189 = (bf16[512,256]{1,0:T(8,128)(2,1)}, bf16[512,256]{1,0:T(8,128)(2,1)}, bf16[512,256]{1,0:T(8,128)(2,1)}, bf16[512,512]{1,0:T(8,128)(2,1)}, bf16[5...) custom-call(s32[1]{0:T(128)} %bitcast.tp_ref, bf16[64,16,512]{2,1,0:T(8,128)(2,1)} %all-to-all-done.refs_0_, ...), custom_call_target="tpu_custom_call" | custom-call | flops 2684354560 | tf_op jit(solution)/shard_map/pallas_call | solution.py:19
  132.4 1.1 fusion.13
  133.5 2.7 collective-permute-start.6
  136.2 14.4 %collective-permute-done.6 = bf16[256,512]{1,0:T(8,128)(2,1)S(1)} collective-permute-done((bf16[256,512]{1,0:T(8,128)(2,1)S(1)}, bf16[256,512]{1,0:T(8,128)(2,1)S(1)}, u32[]{:S(2)}, u32[]{:S(2)}) %collective-permute-start.6) | collective-permute-done | bytes 262176 | tf_op jit(solution)/shard_map/ppermute | solution.py:304
  150.7 1.1 add_convert_fusion.3
  151.8 2.1 collective-permute-start.7
  154.0 1.1 fusion.1
  155.0 15.1 %all-to-all-start.3 = ((bf16[64,8,512]{2,1,0:T(8,128)(2,1)}), bf16[64,8,512]{2,1,0:T(8,128)(2,1)S(1)}, u32[]{:S(2)}, u32[]{:S(2)}) async-start(bf16[64,8,512]{2,1,0:T(8,128)(2,1)} %fusion.1), calls=%async_computation.3 | async-start | bytes 1048576 | tf_op jit(solution)/shard_map/all_to_all | solution.py:275
  170.2 1.1 add_convert_fusion.4
  171.4 14.3 %collective-permute-done.5 = bf16[512,512]{1,0:T(8,128)(2,1)S(1)} collective-permute-done((bf16[512,512]{1,0:T(8,128)(2,1)S(1)}, bf16[512,512]{1,0:T(8,128)(2,1)S(1)}, u32[]{:S(2)}, u32[]{:S(2)}) %collective-permute-start.5) | collective-permute-done | bytes 524320 | tf_op jit(solution)/shard_map/ppermute | solution.py:304
  186.7 11.2 %all-to-all-start.1 = ((bf16[64,8,512]{2,1,0:T(8,128)(2,1)}), bf16[64,8,512]{2,1,0:T(8,128)(2,1)S(1)}, u32[]{:S(2)}, u32[]{:S(2)}) async-start(bf16[64,8,512]{2,1,0:T(8,128)(2,1)} %fusion), calls=%async_computation.1 | async-start | bytes 1048576 | tf_op jit(solution)/shard_map/all_to_all | solution.py:275
  197.9 4.6 %collective-permute-start.18 = (f32[2,256]{1,0:T(2,128)S(1)}, f32[2,256]{1,0:T(2,128)S(1)}, u32[]{:S(2)}, u32[]{:S(2)}) collective-permute-start(f32[2,256]{1,0:T(2,128)S(1)} %slice.67), channel_id=1, source_target_pairs={{0,4},{4,8},{8,12},{12,16},{16,20},{20,24},{24,28},{28,32},{32,36}... | collective-permute-start | bytes 6152 | tf_op jit(solution)/shard_map/ppermute | solution.py:271
  202.5 4.8 %collective-permute-done.18 = f32[2,256]{1,0:T(2,128)S(1)} collective-permute-done((f32[2,256]{1,0:T(2,128)S(1)}, f32[2,256]{1,0:T(2,128)S(1)}, u32[]{:S(2)}, u32[]{:S(2)}) %collective-permute-start.18) | collective-permute-done | bytes 2080 | tf_op jit(solution)/shard_map/ppermute | solution.py:271
  209.7 2.8 all-to-all-done.1.back0
  213.3 2.9 %shard_map.192 = (bf16[256,512]{1,0:T(8,128)(2,1)}, f32[1,256]{1,0:T(1,128)}) custom-call(s32[1]{0:T(128)} %bitcast.tp_ref, bf16[512,256]{1,0:T(8,128)(2,1)} %get-tuple-element.41.pick0, bf16[64,8,512]{2,1,0:T(8,128)(2,1)} %copy-done.4, bf16[512,256]{1,0:T(8,128)(2,1)} %get-tuple-element.47.pick1, bf16[64,8,512]{2,1,0:T(8,128)(2,1)} %copy-done.3, ...), custom_call_target="tpu_custom_call" | custom-call | tf_op jit(solution)/shard_map/pallas_call | solution.py:19
  217.8 1.0 collective-permute-done.15.s1
  218.8 1.5 collective-permute-done.16.s2
  221.9 3.5 %shard_map.193 = (bf16[256,512]{1,0:T(8,128)(2,1)}, f32[256,1]{1,0:T(8,128)}, bf16[16,2,32,256]{3,2,1,0:T(8,128)(2,1)}, bf16[16,2,32,256]{3,2,1,0:T(8,128)(2,1)}) custom-call(s32[1]{0:T(128)} %bitcast.tp_ref, s32[1]{0:T(128)} %bitcast.1.core_ref, bf16[256,512]{1,0:T(8,128)(2,1)} %get-tuple-element.57.token_ref, f32[1,256]{1,0:T(1,128)} %get-tuple-element.58.s0, ...), custom_call_target="tpu_custom_call" | custom-call | tf_op jit(solution)/shard_map/pallas_call | solution.py:19
  225.4 2.5 collective-permute-start.26
  227.9 1.7 collective-permute-done.26
  229.6 2.0 add_convert_fusion
  231.6 10.8 %all-to-all-start.4 = ((bf16[32,32,256]{2,1,0:T(8,128)(2,1)}), bf16[32,32,256]{2,1,0:T(8,128)(2,1)S(1)}, u32[]{:S(2)}, u32[]{:S(2)}) async-start(bf16[32,32,256]{2,1,0:T(8,128)(2,1)} %bitcast.10), calls=%async_computation.4 | async-start | bytes 1048576 | tf_op jit(solution)/shard_map/all_to_all | solution.py:275
  243.1 1.1 collective-permute-start.23
  244.2 9.9 %shard_map.195 = (f32[1,2048,256]{2,1,0:T(8,128)}, f32[1,2048,256]{2,1,0:T(8,128)}, f32[1,256,2048]{2,1,0:T(8,128)}) custom-call(s32[1]{0:T(128)} %bitcast.tp_ref, bf16[64,16,512]{2,1,0:T(8,128)(2,1)} %all-to-all-done.refs_0_, bf16[64,16,512]{2,1,0:T(8,128)(2,1)} %copy-done.16, bf16[64,16,512]{2,1,0:T(8,128)(2,1)} %copy-done.15, ...), custom_call_target="tpu_custom_call" | custom-call | flops 3221225472 | tf_op jit(solution)/shard_map/pallas_call | solution.py:19
  254.2 4.3 %collective-permute-done.24.t3 = bf16[256,512]{1,0:T(8,128)(2,1)S(1)} collective-permute-done((bf16[256,512]{1,0:T(8,128)(2,1)S(1)}, bf16[256,512]{1,0:T(8,128)(2,1)S(1)}, u32[]{:S(2)}, u32[]{:S(2)}) %collective-permute-start.24) | collective-permute-done | bytes 262176 | tf_op jit(solution)/shard_map/ppermute | solution.py:304
  259.1 3.8 %shard_map.194 = (bf16[256,256]{1,0:T(8,128)(2,1)}, f32[256,256]{1,0:T(8,128)}) custom-call(s32[1]{0:T(128)} %bitcast.tp_ref, bf16[256,512]{1,0:T(8,128)(2,1)} %get-tuple-element.91.g0, bf16[256,512]{1,0:T(8,128)(2,1)} %copy-done.12, bf16[256,512]{1,0:T(8,128)(2,1)} %copy-done.13, bf16[256,512]{1,0:T(8,128)(2,1)} %copy-done.14, ...), custom_call_target="tpu_custom_call" | custom-call | tf_op jit(solution)/shard_map/pallas_call | solution.py:19
  263.6 2.4 collective-permute-start.25
  267.0 4.8 %collective-permute-done.25 = f32[2,256]{1,0:T(2,128)S(1)} collective-permute-done((f32[2,256]{1,0:T(2,128)S(1)}, f32[2,256]{1,0:T(2,128)S(1)}, u32[]{:S(2)}, u32[]{:S(2)}) %collective-permute-start.25) | collective-permute-done | bytes 2080 | tf_op jit(solution)/shard_map/ppermute | solution.py:271
  271.9 1.7 fusion.6
  273.6 1.9 collective-permute-start.27
  276.3 8.3 %collective-permute-done.27 = f32[32,256]{1,0:T(8,128)S(1)} collective-permute-done((f32[32,256]{1,0:T(8,128)S(1)}, f32[32,256]{1,0:T(8,128)S(1)}, u32[]{:S(2)}, u32[]{:S(2)}) %collective-permute-start.27) | collective-permute-done | bytes 32800 | tf_op jit(solution)/shard_map/ppermute | solution.py:420
  (96 shorter events, 15.8 us)
Async XLA Ops:
  41.5 38.4 %copy-start = (bf16[64,16,512]{2,1,0:T(8,128)(2,1)}, bf16[64,16,512]{2,1,0:T(8,128)(2,1)S(1)}, u32[]{:S(2)}) copy-start(bf16[64,16,512]{2,1,0:T(8,128)(2,1)S(1)} %all_to_all.25.own.refs_8_) | copy-start | bytes 3145732
  41.5 34.6 %all-to-all-start = ((bf16[64,16,512]{2,1,0:T(8,128)(2,1)}), bf16[64,16,512]{2,1,0:T(8,128)(2,1)}, u32[]{:S(2)}, u32[]{:S(2)}) async-start(bf16[64,16,512]{2,1,0:T(8,128)(2,1)} %get-tuple-element.42), calls=%async_computation | async-start | bytes 2097152 | tf_op jit(solution)/shard_map/all_to_all | solution.py:275
  50.3 28.4 %collective-permute-start.8 = (bf16[64,16,512]{2,1,0:T(8,128)(2,1)S(1)}, bf16[64,16,512]{2,1,0:T(8,128)(2,1)S(1)}, u32[]{:S(2)}, u32[]{:S(2)}) collective-permute-start(bf16[64,16,512]{2,1,0:T(8,128)(2,1)S(1)} %all_to_all.25.own.refs_8_), channel_id=1, source_target_pairs={{0,1},{1,2},{2,3},{3,0},{4,5},{5,6},{6,7},{7,4},{8,9},{9,10},{10,1... | collective-permute-start | bytes 3145736 | tf_op jit(solution)/shard_map/ppermute | solution.py:304
  51.5 27.3 %collective-permute-start.10 = (bf16[64,16,512]{2,1,0:T(8,128)(2,1)S(1)}, bf16[64,16,512]{2,1,0:T(8,128)(2,1)S(1)}, u32[]{:S(2)}, u32[]{:S(2)}) collective-permute-start(bf16[64,16,512]{2,1,0:T(8,128)(2,1)S(1)} %all_to_all.25.own.refs_8_), channel_id=1, source_target_pairs={{0,3},{1,0},{2,1},{3,2},{4,7},{5,4},{6,5},{7,6},{8,11},{9,8},{10,9... | collective-permute-start | bytes 3145736 | tf_op jit(solution)/shard_map/ppermute | solution.py:304
  76.0 25.3 %collective-permute-start.1 = (bf16[64,16,512]{2,1,0:T(8,128)(2,1)}, bf16[64,16,512]{2,1,0:T(8,128)(2,1)S(1)}, u32[]{:S(2)}, u32[]{:S(2)}) collective-permute-start(bf16[64,16,512]{2,1,0:T(8,128)(2,1)} %all-to-all-done.refs_0_), channel_id=1, source_target_pairs={{0,1},{1,2},{2,3},{3,0},{4,5},{5,6},{6,7},{7,4},{8,9},{9,10},{10,1... | collective-permute-start | bytes 3145736 | tf_op jit(solution)/shard_map/ppermute | solution.py:304
  77.2 25.9 %collective-permute-start = (bf16[64,16,512]{2,1,0:T(8,128)(2,1)}, bf16[64,16,512]{2,1,0:T(8,128)(2,1)S(1)}, u32[]{:S(2)}, u32[]{:S(2)}) collective-permute-start(bf16[64,16,512]{2,1,0:T(8,128)(2,1)} %all-to-all-done.refs_0_), channel_id=1, source_target_pairs={{0,3},{1,0},{2,1},{3,2},{4,7},{5,4},{6,5},{7,6},{8,11},{9,8},{10,9... | collective-permute-start | bytes 3145736 | tf_op jit(solution)/shard_map/ppermute | solution.py:304
  78.7 26.2 %copy-start.1 = (bf16[64,16,512]{2,1,0:T(8,128)(2,1)}, bf16[64,16,512]{2,1,0:T(8,128)(2,1)S(1)}, u32[]{:S(2)}) copy-start(bf16[64,16,512]{2,1,0:T(8,128)(2,1)S(1)} %collective-permute-done.8.before.refs_10_) | copy-start | bytes 3145732
  78.7 34.3 %collective-permute-start.9 = (bf16[64,8,512]{2,1,0:T(8,128)(2,1)S(1)}, bf16[64,8,512]{2,1,0:T(8,128)(2,1)}, u32[]{:S(2)}, u32[]{:S(2)}) collective-permute-start(bf16[64,8,512]{2,1,0:T(8,128)(2,1)S(1)} %slice.65), channel_id=1, source_target_pairs={{0,1},{1,2},{2,3},{3,0},{4,5},{5,6},{6,7},{7,4},{8,9},{9,10},{10,1... | collective-permute-start | bytes 1572872 | tf_op jit(solution)/shard_map/ppermute | solution.py:304
  78.8 28.8 %copy-start.2 = (bf16[64,16,512]{2,1,0:T(8,128)(2,1)}, bf16[64,16,512]{2,1,0:T(8,128)(2,1)S(1)}, u32[]{:S(2)}) copy-start(bf16[64,16,512]{2,1,0:T(8,128)(2,1)S(1)} %collective-permute-done.10.after.refs_9_) | copy-start | bytes 3145732
  79.8 33.2 %collective-permute-start.11 = (bf16[64,8,512]{2,1,0:T(8,128)(2,1)}, bf16[64,8,512]{2,1,0:T(8,128)(2,1)}, u32[]{:S(2)}, u32[]{:S(2)}) collective-permute-start(bf16[64,8,512]{2,1,0:T(8,128)(2,1)} %slice.66), channel_id=1, source_target_pairs={{0,3},{1,0},{2,1},{3,2},{4,7},{5,4},{6,5},{7,6},{8,11},{9,8},{10,9... | collective-permute-start | bytes 1572872 | tf_op jit(solution)/shard_map/ppermute | solution.py:304
  103.1 20.8 %collective-permute-start.2 = (bf16[64,8,512]{2,1,0:T(8,128)(2,1)}, bf16[64,8,512]{2,1,0:T(8,128)(2,1)}, u32[]{:S(2)}, u32[]{:S(2)}) collective-permute-start(bf16[64,8,512]{2,1,0:T(8,128)(2,1)} %slice.63), channel_id=1, source_target_pairs={{0,1},{1,2},{2,3},{3,0},{4,5},{5,6},{6,7},{7,4},{8,9},{9,10},{10,1... | collective-permute-start | bytes 1572872 | tf_op jit(solution)/shard_map/ppermute | solution.py:304
  104.9 18.9 %collective-permute-start.3 = (bf16[64,8,512]{2,1,0:T(8,128)(2,1)}, bf16[64,8,512]{2,1,0:T(8,128)(2,1)}, u32[]{:S(2)}, u32[]{:S(2)}) collective-permute-start(bf16[64,8,512]{2,1,0:T(8,128)(2,1)} %slice.64), channel_id=1, source_target_pairs={{0,3},{1,0},{2,1},{3,2},{4,7},{5,4},{6,5},{7,6},{8,11},{9,8},{10,9... | collective-permute-start | bytes 1572872 | tf_op jit(solution)/shard_map/ppermute | solution.py:304
  119.0 35.0 %collective-permute-start.14 = (bf16[512,512]{1,0:T(8,128)(2,1)}, bf16[512,512]{1,0:T(8,128)(2,1)S(1)}, u32[]{:S(2)}, u32[]{:S(2)}) collective-permute-start(bf16[512,512]{1,0:T(8,128)(2,1)} %get-tuple-element.55), channel_id=1, source_target_pairs={{0,2},{1,3},{2,0},{3,1},{4,6},{5,7},{6,4},{7,5},{8,10},{9,11},{10,... | collective-permute-start | bytes 1572872 | tf_op jit(solution)/shard_map/ppermute | solution.py:304
  120.7 33.3 %collective-permute-start.13 = (bf16[512,512]{1,0:T(8,128)(2,1)}, bf16[512,512]{1,0:T(8,128)(2,1)S(1)}, u32[]{:S(2)}, u32[]{:S(2)}) collective-permute-start(bf16[512,512]{1,0:T(8,128)(2,1)} %get-tuple-element.54), channel_id=1, source_target_pairs={{0,3},{1,0},{2,1},{3,2},{4,7},{5,4},{6,5},{7,6},{8,11},{9,8},{10,9... | collective-permute-start | bytes 1572872 | tf_op jit(solution)/shard_map/ppermute | solution.py:304
  121.9 32.1 %collective-permute-start.12 = (bf16[512,512]{1,0:T(8,128)(2,1)}, bf16[512,512]{1,0:T(8,128)(2,1)S(1)}, u32[]{:S(2)}, u32[]{:S(2)}) collective-permute-start(bf16[512,512]{1,0:T(8,128)(2,1)} %get-tuple-element.53), channel_id=1, source_target_pairs={{0,1},{1,2},{2,3},{3,0},{4,5},{5,6},{6,7},{7,4},{8,9},{9,10},{10,1... | collective-permute-start | bytes 1572872 | tf_op jit(solution)/shard_map/ppermute | solution.py:304
  132.4 21.6 %copy-start.5 = (bf16[512,512]{1,0:T(8,128)(2,1)S(1)}, bf16[512,512]{1,0:T(8,128)(2,1)}, u32[]{:S(2)}) copy-start(bf16[512,512]{1,0:T(8,128)(2,1)} %get-tuple-element.52) | copy-start | bytes 1572868
  133.5 17.2 %collective-permute-start.6 = (bf16[256,512]{1,0:T(8,128)(2,1)S(1)}, bf16[256,512]{1,0:T(8,128)(2,1)S(1)}, u32[]{:S(2)}, u32[]{:S(2)}) collective-permute-start(bf16[256,512]{1,0:T(8,128)(2,1)S(1)} %get-tuple-element.79), channel_id=1, source_target_pairs={{0,3},{1,0},{2,1},{3,2},{4,7},{5,4},{6,5},{7,6},{8,11},{9,8},{10,9... | collective-permute-start | bytes 786440 | tf_op jit(solution)/shard_map/ppermute | solution.py:304
  136.2 33.9 %collective-permute-start.4 = (bf16[256,512]{1,0:T(8,128)(2,1)S(1)}, bf16[256,512]{1,0:T(8,128)(2,1)}, u32[]{:S(2)}, u32[]{:S(2)}) collective-permute-start(bf16[256,512]{1,0:T(8,128)(2,1)S(1)} %get-tuple-element.78), channel_id=1, source_target_pairs={{0,1},{1,2},{2,3},{3,0},{4,5},{5,6},{6,7},{7,4},{8,9},{9,10},{10,1... | collective-permute-start | bytes 786440 | tf_op jit(solution)/shard_map/ppermute | solution.py:304
  151.8 18.3 %copy-start.6 = (bf16[512,512]{1,0:T(8,128)(2,1)S(1)}, bf16[512,512]{1,0:T(8,128)(2,1)}, u32[]{:S(2)}) copy-start(bf16[512,512]{1,0:T(8,128)(2,1)} %get-tuple-element.44) | copy-start | bytes 1572868
  151.8 19.5 %collective-permute-start.7 = (bf16[512,512]{1,0:T(8,128)(2,1)S(1)}, bf16[512,512]{1,0:T(8,128)(2,1)S(1)}, u32[]{:S(2)}, u32[]{:S(2)}) collective-permute-start(bf16[512,512]{1,0:T(8,128)(2,1)S(1)} %add_convert_fusion.3), channel_id=1, source_target_pairs={{0,3},{1,0},{2,1},{3,2},{4,7},{5,4},{6,5},{7,6},{8,11},{9,8},{10,9... | collective-permute-start | bytes 1572872 | tf_op jit(solution)/shard_map/ppermute | solution.py:304
  154.0 31.7 %copy-start.10 = (bf16[512,512]{1,0:T(8,128)(2,1)S(1)}, bf16[512,512]{1,0:T(8,128)(2,1)}, u32[]{:S(2)}) copy-start(bf16[512,512]{1,0:T(8,128)(2,1)} %get-tuple-element.43) | copy-start | bytes 1572868
  155.0 31.6 %all-to-all-start.3 = ((bf16[64,8,512]{2,1,0:T(8,128)(2,1)}), bf16[64,8,512]{2,1,0:T(8,128)(2,1)S(1)}, u32[]{:S(2)}, u32[]{:S(2)}) async-start(bf16[64,8,512]{2,1,0:T(8,128)(2,1)} %fusion.1), calls=%async_computation.3 | async-start | bytes 1048576 | tf_op jit(solution)/shard_map/all_to_all | solution.py:275
  170.1 27.7 %copy-start.8 = (bf16[256,256]{1,0:T(8,128)(2,1)S(1)}, bf16[256,256]{1,0:T(8,128)(2,1)}, u32[]{:S(2)}) copy-start(bf16[256,256]{1,0:T(8,128)(2,1)} %param.17) | copy-start | bytes 393220
  170.2 27.7 %copy-start.11 = (bf16[256,256]{1,0:T(8,128)(2,1)S(1)}, bf16[256,256]{1,0:T(8,128)(2,1)}, u32[]{:S(2)}) copy-start(bf16[256,256]{1,0:T(8,128)(2,1)} %param.18) | copy-start | bytes 393220
  171.2 31.2 %copy-start.21 = (f32[3,256]{1,0:T(4,128)S(1)}, f32[3,256]{1,0:T(4,128)}, u32[]{:S(2)}) copy-start(f32[3,256]{1,0:T(4,128)} %param.19) | copy-start | bytes 9220
  171.3 36.1 %copy-start.7 = (bf16[256,256]{1,0:T(8,128)(2,1)S(1)}, bf16[256,256]{1,0:T(8,128)(2,1)}, u32[]{:S(2)}) copy-start(bf16[256,256]{1,0:T(8,128)(2,1)} %gate_ref.3) | copy-start | bytes 393220
  171.3 14.4 %collective-permute-start.5 = (bf16[512,512]{1,0:T(8,128)(2,1)S(1)}, bf16[512,512]{1,0:T(8,128)(2,1)S(1)}, u32[]{:S(2)}, u32[]{:S(2)}) collective-permute-start(bf16[512,512]{1,0:T(8,128)(2,1)S(1)} %add_convert_fusion.4), channel_id=1, source_target_pairs={{0,1},{1,2},{2,3},{3,0},{4,5},{5,6},{6,7},{7,4},{8,9},{9,10},{10,1... | collective-permute-start | bytes 1572872 | tf_op jit(solution)/shard_map/ppermute | solution.py:304
  186.7 25.9 %copy-start.3 = (bf16[64,8,512]{2,1,0:T(8,128)(2,1)}, bf16[64,8,512]{2,1,0:T(8,128)(2,1)S(1)}, u32[]{:S(2)}) copy-start(bf16[64,8,512]{2,1,0:T(8,128)(2,1)S(1)} %all-to-all-done.3.back1) | copy-start | bytes 1572868
  186.7 25.8 %all-to-all-start.1 = ((bf16[64,8,512]{2,1,0:T(8,128)(2,1)}), bf16[64,8,512]{2,1,0:T(8,128)(2,1)S(1)}, u32[]{:S(2)}, u32[]{:S(2)}) async-start(bf16[64,8,512]{2,1,0:T(8,128)(2,1)} %fusion), calls=%async_computation.1 | async-start | bytes 1048576 | tf_op jit(solution)/shard_map/all_to_all | solution.py:275
  197.9 9.5 %collective-permute-start.18 = (f32[2,256]{1,0:T(2,128)S(1)}, f32[2,256]{1,0:T(2,128)S(1)}, u32[]{:S(2)}, u32[]{:S(2)}) collective-permute-start(f32[2,256]{1,0:T(2,128)S(1)} %slice.67), channel_id=1, source_target_pairs={{0,4},{4,8},{8,12},{12,16},{16,20},{20,24},{24,28},{28,32},{32,36}... | collective-permute-start | bytes 6152 | tf_op jit(solution)/shard_map/ppermute | solution.py:271
  208.2 13.1 %copy-start.9 = (bf16[256,256]{1,0:T(8,128)(2,1)}, bf16[256,256]{1,0:T(8,128)(2,1)S(1)}, u32[]{:S(2)}) copy-start(bf16[256,256]{1,0:T(8,128)(2,1)S(1)} %get-tuple-element.76.m0) | copy-start | bytes 393220
  208.2 8.8 %collective-permute-start.19 = (bf16[256,256]{1,0:T(8,128)(2,1)S(1)}, bf16[256,256]{1,0:T(8,128)(2,1)S(1)}, u32[]{:S(2)}, u32[]{:S(2)}) collective-permute-start(bf16[256,256]{1,0:T(8,128)(2,1)S(1)} %get-tuple-element.76.m0), channel_id=1, source_target_pairs={{0,3},{1,0},{2,1},{3,2},{4,7},{5,4},{6,5},{7,6},{8,11},{9,8},{10,9... | collective-permute-start | bytes 393224 | tf_op jit(solution)/shard_map/ppermute | solution.py:304
  208.2 9.6 %collective-permute-start.20 = (bf16[256,256]{1,0:T(8,128)(2,1)S(1)}, bf16[256,256]{1,0:T(8,128)(2,1)S(1)}, u32[]{:S(2)}, u32[]{:S(2)}) collective-permute-start(bf16[256,256]{1,0:T(8,128)(2,1)S(1)} %get-tuple-element.76.m0), channel_id=1, source_target_pairs={{0,2},{1,3},{2,0},{3,1},{4,6},{5,7},{6,4},{7,5},{8,10},{9,11},{10,... | collective-permute-start | bytes 393224 | tf_op jit(solution)/shard_map/ppermute | solution.py:304
  208.8 9.0 %collective-permute-start.21 = (bf16[256,256]{1,0:T(8,128)(2,1)S(1)}, bf16[256,256]{1,0:T(8,128)(2,1)S(1)}, u32[]{:S(2)}, u32[]{:S(2)}) collective-permute-start(bf16[256,256]{1,0:T(8,128)(2,1)S(1)} %get-tuple-element.76.m0), channel_id=1, source_target_pairs={{0,1},{1,2},{2,3},{3,0},{4,5},{5,6},{6,7},{7,4},{8,9},{9,10},{10,1... | collective-permute-start | bytes 393224 | tf_op jit(solution)/shard_map/ppermute | solution.py:304
  216.2 2.6 collective-permute-start.15
  216.2 4.2 %collective-permute-start.16 = (f32[1,256]{1,0:T(1,128)}, f32[1,256]{1,0:T(1,128)S(1)}, u32[]{:S(2)}, u32[]{:S(2)}) collective-permute-start(f32[1,256]{1,0:T(1,128)} %get-tuple-element.58.s0), channel_id=1, source_target_pairs={{0,2},{1,3},{2,0},{3,1},{4,6},{5,7},{6,4},{7,5},{8,10},{9,11},{10,... | collective-permute-start | bytes 3080 | tf_op jit(solution)/shard_map/ppermute | solution.py:304
  217.0 4.3 %copy-start.18 = (bf16[256,256]{1,0:T(8,128)(2,1)}, bf16[256,256]{1,0:T(8,128)(2,1)S(1)}, u32[]{:S(2)}) copy-start(bf16[256,256]{1,0:T(8,128)(2,1)S(1)} %collective-permute-done.19.m1) | copy-start | bytes 393220
  217.0 4.3 %collective-permute-start.17 = (f32[1,256]{1,0:T(1,128)}, f32[1,256]{1,0:T(1,128)S(1)}, u32[]{:S(2)}, u32[]{:S(2)}) collective-permute-start(f32[1,256]{1,0:T(1,128)} %get-tuple-element.58.s0), channel_id=1, source_target_pairs={{0,1},{1,2},{2,3},{3,0},{4,5},{5,6},{6,7},{7,4},{8,9},{9,10},{10,1... | collective-permute-start | bytes 3080 | tf_op jit(solution)/shard_map/ppermute | solution.py:304
  221.9 20.6 %copy-start.17 = (bf16[256,512]{1,0:T(8,128)(2,1)S(1)}, bf16[256,512]{1,0:T(8,128)(2,1)}, u32[]{:S(2)}) copy-start(bf16[256,512]{1,0:T(8,128)(2,1)} %get-tuple-element.57.token_ref) | copy-start | bytes 786436
  225.4 4.2 %collective-permute-start.26 = (bf16[16,2,32,256]{3,2,1,0:T(8,128)(2,1)}, bf16[16,2,32,256]{3,2,1,0:T(8,128)(2,1)S(1)}, u32[]{:S(2)}, u32[]{:S(2)}) collective-permute-start(bf16[16,2,32,256]{3,2,1,0:T(8,128)(2,1)} %get-tuple-element.64), channel_id=1, source_target_pairs={{0,4},{4,0},{8,12},{12,8},{16,20},{20,16},{24,28},{28,24},{32,36},... | collective-permute-start | bytes 1572872 | tf_op jit(solution)/shard_map/ppermute | solution.py:409
  231.6 41.9 %all-to-all-start.4 = ((bf16[32,32,256]{2,1,0:T(8,128)(2,1)}), bf16[32,32,256]{2,1,0:T(8,128)(2,1)S(1)}, u32[]{:S(2)}, u32[]{:S(2)}) async-start(bf16[32,32,256]{2,1,0:T(8,128)(2,1)} %bitcast.10), calls=%async_computation.4 | async-start | bytes 1048576 | tf_op jit(solution)/shard_map/all_to_all | solution.py:275
  242.5 11.7 %collective-permute-start.22 = (bf16[256,512]{1,0:T(8,128)(2,1)S(1)}, bf16[256,512]{1,0:T(8,128)(2,1)S(1)}, u32[]{:S(2)}, u32[]{:S(2)}) collective-permute-start(bf16[256,512]{1,0:T(8,128)(2,1)S(1)} %copy-done.17), channel_id=1, source_target_pairs={{0,3},{1,0},{2,1},{3,2},{4,7},{5,4},{6,5},{7,6},{8,11},{9,8},{10,9... | collective-permute-start | bytes 786440 | tf_op jit(solution)/shard_map/ppermute | solution.py:304
  243.1 11.1 %collective-permute-start.23 = (bf16[256,512]{1,0:T(8,128)(2,1)S(1)}, bf16[256,512]{1,0:T(8,128)(2,1)S(1)}, u32[]{:S(2)}, u32[]{:S(2)}) collective-permute-start(bf16[256,512]{1,0:T(8,128)(2,1)S(1)} %copy-done.17), channel_id=1, source_target_pairs={{0,2},{1,3},{2,0},{3,1},{4,6},{5,7},{6,4},{7,5},{8,10},{9,11},{10,... | collective-permute-start | bytes 786440 | tf_op jit(solution)/shard_map/ppermute | solution.py:304
  244.2 14.2 %collective-permute-start.24 = (bf16[256,512]{1,0:T(8,128)(2,1)S(1)}, bf16[256,512]{1,0:T(8,128)(2,1)S(1)}, u32[]{:S(2)}, u32[]{:S(2)}) collective-permute-start(bf16[256,512]{1,0:T(8,128)(2,1)S(1)} %copy-done.17), channel_id=1, source_target_pairs={{0,1},{1,2},{2,3},{3,0},{4,5},{5,6},{6,7},{7,4},{8,9},{9,10},{10,1... | collective-permute-start | bytes 786440 | tf_op jit(solution)/shard_map/ppermute | solution.py:304
  254.1 4.3 %copy-start.12 = (bf16[256,512]{1,0:T(8,128)(2,1)}, bf16[256,512]{1,0:T(8,128)(2,1)S(1)}, u32[]{:S(2)}) copy-start(bf16[256,512]{1,0:T(8,128)(2,1)S(1)} %collective-permute-done.22.t1) | copy-start | bytes 786436
  254.2 4.3 %copy-start.13 = (bf16[256,512]{1,0:T(8,128)(2,1)}, bf16[256,512]{1,0:T(8,128)(2,1)S(1)}, u32[]{:S(2)}) copy-start(bf16[256,512]{1,0:T(8,128)(2,1)S(1)} %collective-permute-done.23.t2) | copy-start | bytes 786436
  263.6 8.2 %collective-permute-start.25 = (f32[2,256]{1,0:T(2,128)S(1)}, f32[2,256]{1,0:T(2,128)S(1)}, u32[]{:S(2)}, u32[]{:S(2)}) collective-permute-start(f32[2,256]{1,0:T(2,128)S(1)} %slice.60), channel_id=1, source_target_pairs={{4,0},{8,4},{12,8},{16,12},{20,16},{24,20},{28,24},{32,28},{36,32}... | collective-permute-start | bytes 6152 | tf_op jit(solution)/shard_map/ppermute | solution.py:271
  273.6 10.9 %collective-permute-start.27 = (f32[32,256]{1,0:T(8,128)S(1)}, f32[32,256]{1,0:T(8,128)S(1)}, u32[]{:S(2)}, u32[]{:S(2)}) collective-permute-start(f32[32,256]{1,0:T(8,128)S(1)} %convert_reduce_fusion), channel_id=1, source_target_pairs={{0,0},{1,64},{2,128},{3,192},{4,1},{5,65},{6,129},{7,193},{8,2},{9... | collective-permute-start | bytes 98312 | tf_op jit(solution)/shard_map/ppermute | solution.py:420
  (9 other events, 14.4 us)
where the time goes:
time: 286 us; the launch traced here: 285 us
  waiting for transfers between devices  103 us (36%)
  starting transfers between devices  80.9 us (28%)
  Pallas kernels  44.1 us (15%)
  blocking collectives  36.7 us (13%)
  local copies, waits for them, and re-layouts  10.2 us (4%)
  other arithmetic  9.61 us (3%)
    ppermute x24, waiting for transfers between devices, send_along(): return lax.ppermute(value, 'tp', pairs)  57 us
    all_to_all x4, starting transfers between devices, exchange(): lax.all_to_all(array, axis, split_axis=0, concat_axis=0, tiled=True, axis...  45.9 us
    pallas_call x8, Pallas kernels, call(): pl.pallas_call(body, out_shape=[jax.ShapeDtypeStruct(shape, dtype) for sh...  44.1 us
    all_to_all x1, blocking collectives, exchange(): lax.all_to_all(array, axis, split_axis=0, concat_axis=0, tiled=True, axis...  36.7 us
    all_to_all x4, waiting for transfers between devices, exchange(): lax.all_to_all(array, axis, split_axis=0, concat_axis=0, tiled=True, axis...  25.8 us
    ppermute x24, starting transfers between devices, send_along(): return lax.ppermute(value, 'tp', pairs)  23.7 us
    ppermute x2, waiting for transfers between devices, shift_edge(): lax.ppermute(value, axis, [(source, source + steps) for source in range(f...  9.68 us
    ppermute x1, waiting for transfers between devices, body(): grad_out_weight = lax.ppermute(reduced, ('sp', 'tp'), placed)  8.33 us
  transfers between devices with their start and end apart: 32, of which 14 were waited for; matrix products, arithmetic and copies ran while one was open for 5% of the time, Pallas kernels for 13%

commit v1 on v0

--- a/solution.py
+++ b/solution.py
@@ -36,7 +36,9 @@
     return [(k, (k + steps) % size) for k in range(size)]
 
 
-def send_kernel(tp_ref, choice_ref, scale_ref, stream_ref, gain_ref, cot_ref, rms_ref, *outs):
+def send_kernel(
+    tp_ref, choice_ref, scale_ref, stream_ref, gain_ref, cot_ref, rms_ref, weight_ref, *outs
+):
     tokens, _ = stream_ref.shape
     chunks = len(outs) // 2
     experts, part, columns = outs[0].shape
@@ -73,9 +75,27 @@
             pick_second, scale_ref[1:2, :], 0.0
         )
         weight = jnp.sum(scale, axis=1, keepdims=True)
+        if c == chunks - 1:
+            weight_ref[...] = weight
         send_ref[:, part:, :] = (
             (dot(pick, cot, (1, 0)) * weight).astype(bf16).reshape(experts, part, columns)
         )
+
+
+def send_far_kernel(
+    tp_ref, pick_ref, weight_ref, rms_ref, stream_ref, gain_ref, cot_ref, send_ref
+):
+    experts, part, columns = send_ref.shape
+    part = part // 2
+    here = pl.ds(column_starts(tp_ref, columns)[2], columns)
+    pick = pick_ref[...]
+    normed = (stream_ref[:, here].astype(f32) * rms_ref[...] * gain_ref[:, here]).astype(bf16)
+    send_ref[:, :part, :] = dot(pick, normed, (1, 0)).astype(bf16).reshape(experts, part, columns)
+    send_ref[:, part:, :] = (
+        (dot(pick, cot_ref[:, here], (1, 0)) * weight_ref[...])
+        .astype(bf16)
+        .reshape(experts, part, columns)
+    )
 
 
 def block(ref, k, parts=2, half=None):
@@ -87,11 +107,11 @@
 
 
 def gathered_blocks(refs, half=None):
-    own, after, before, far_rows, far_scaled = refs
-    rows = [block(r, 0, p, half) for r, p in ((own, 2), (after, 2), (far_rows, 1), (before, 2))]
+    own, after, before, *far = refs
+    far = [(far[0], 0, 2), (far[0], 1, 2)] if len(far) == 1 else [(far[0], 0, 1), (far[1], 0, 1)]
+    rows = [block(r, k, p, half) for r, k, p in ((own, 0, 2), (after, 0, 2), far[0], (before, 0, 2))]
     scaled = [
-        block(r, k, p, half)
-        for r, k, p in ((own, 1, 2), (after, 1, 2), (far_scaled, 0, 1), (before, 1, 2))
+        block(r, k, p, half) for r, k, p in ((own, 1, 2), (after, 1, 2), far[1], (before, 1, 2))
     ]
     return rows, scaled
 
@@ -134,22 +154,23 @@
 
 
 def expert_kernel(tp_ref, *refs):
-    weights, outs = refs[5:8], refs[8:]
+    given = len(refs) - 10
+    weights, outs = refs[given : given + 3], refs[given + 3 :]
     gate_ref, up_ref, _ = weights
     hidden_ref, ggrad_ref, ugrad_ref, *places = outs
     starts = column_starts(tp_ref, refs[0].shape[2])
     columns = refs[0].shape[2]
 
     def step(half, here):
-        if len(refs[4].shape) == 3:
+        if given == 5:
             rows, scaled = gathered_blocks(refs[:5], half)
             gate_pre, up_pre, hidden_grad = first_products(rows, scaled, *weights, starts)
         else:
             far = first_products(
-                [block(refs[0], 0, 1, half)], [block(refs[1], 0, 1, half)], *weights, starts[2:3]
+                [block(refs[0], 0, 2, half)], [block(refs[0], 1, 2, half)], *weights, starts[2:3]
             )
             gate_pre, up_pre, hidden_grad = (
-                ref[here, :] + value for ref, value in zip(refs[2:5], far)
+                ref[here, :] + value for ref, value in zip(refs[1:4], far)
             )
         sigmoid_gate = jax.nn.sigmoid(gate_pre)
         silu_gate = gate_pre * sigmoid_gate
@@ -170,8 +191,8 @@
 
 
 def weights_kernel(tp_ref, *refs):
-    chunks = (len(refs) - 3) // 8
     outs = refs[-3:]
+    groups = ((refs[:5], refs[5:8]), (refs[8:12], refs[12:15]))
     columns = refs[0].shape[2]
     starts = column_starts(tp_ref, columns)
     part = refs[0].shape[1] // 2
@@ -179,15 +200,14 @@
     def step(half, here):
         for j in range(4):
             gate = up = down = 0.0
-            for c in range(chunks):
-                own, after, before, far_rows, far_scaled = refs[8 * c : 8 * c + 5]
-                ref = (own, after, far_rows, before)[j]
+            for (own, after, before, *far), results in groups:
+                ref = (own, after, far[0], before)[j]
                 rows = ref[:, :part, here].reshape(-1, columns // 2)
-                if j == 2:
-                    scaled = far_scaled[:, :, here].reshape(-1, columns // 2)
+                if j == 2 and len(far) == 2:
+                    scaled = far[1][:, :, here].reshape(-1, columns // 2)
                 else:
                     scaled = ref[:, part:, here].reshape(-1, columns // 2)
-                hidden, gate_grad, up_grad = (refs[8 * c + 5 + k][...] for k in range(3))
+                hidden, gate_grad, up_grad = (r[...] for r in results)
                 gate = gate + dot(rows, gate_grad, (0, 0))
                 up = up + dot(rows, up_grad, (0, 0))
                 down = down + dot(hidden, scaled, (0, 0))
@@ -293,24 +313,35 @@
     gain = norm_gain.reshape(1, width)
 
     sent_block = ((sp_size, 2 * part, columns), bf16)
-    inverse_rms, *sent = call(
+    inverse_rms, far_weight, *sent = call(
         send_kernel,
-        [((tokens, 1), f32)] + [sent_block, ((sp_size * part, tokens), bf16)] * chunks,
+        [((tokens, 1), f32), ((sp_size * part, 1), f32)]
+        + [sent_block, ((sp_size * part, tokens), bf16)] * chunks,
         [tp, expert_choice.T, route_scale.T, stream_in, gain, cotangent],
     )
     picks = sent[1::2]
 
     def send_along(value, pairs):
         return lax.ppermute(value, "tp", pairs)
+
+    (sent_far,) = call(
+        send_far_kernel,
+        [sent_block],
+        [tp, picks[1], far_weight, inverse_rms, stream_in, gain, cotangent],
+    )
 
     gathered = []
     for c in range(chunks):
         own = exchange(sent[2 * c], "sp")
         before = send_along(own, right)
         after = send_along(own, left)
-        far_rows = send_along(before[:, :part], right)
-        far_scaled = send_along(after[:, part:], left)
-        gathered.append([own, after, before, far_rows, far_scaled])
+        if c == 0:
+            far_rows = send_along(before[:, :part], right)
+            far_scaled = send_along(after[:, part:], left)
+            far = [far_rows, far_scaled]
+        else:
+            far = [exchange(sent_far, "sp")]
+        gathered.append([own, after, before, *far])
 
     returned = []
     saved = []

time: 286 us -> 304 us (1.063)
  the two profiles are of different devices: /device:TPU:121 before, /device:TPU:1 now
where the time goes in v1:
time: 304 us; the launch traced here: 298 us
  waiting for transfers between devices  114 us (38%)
  starting transfers between devices  75.4 us (25%)
  Pallas kernels  47.4 us (16%)
  blocking collectives  41.4 us (14%)
  local copies, waits for them, and re-layouts  9.77 us (3%)
  other arithmetic  8.52 us (3%)
    ppermute x22, waiting for transfers between devices, send_along(): return lax.ppermute(value, 'tp', pairs)  69.6 us
    pallas_call x9, Pallas kernels, call(): pl.pallas_call(body, out_shape=[jax.ShapeDtypeStruct(shape, dtype) for sh...  47.4 us
    all_to_all x5, starting transfers between devices, exchange(): lax.all_to_all(array, axis, split_axis=0, concat_axis=0, tiled=True, axis...  44.5 us
    all_to_all x1, blocking collectives, exchange(): lax.all_to_all(array, axis, split_axis=0, concat_axis=0, tiled=True, axis...  41.4 us
    all_to_all x5, waiting for transfers between devices, exchange(): lax.all_to_all(array, axis, split_axis=0, concat_axis=0, tiled=True, axis...  36.7 us
    ppermute x22, starting transfers between devices, send_along(): return lax.ppermute(value, 'tp', pairs)  21.3 us
  transfers between devices with their start and end apart: 31, of which 18 were waited for; matrix products, arithmetic and copies ran while one was open for 4% of the time, Pallas kernels for 13%

profile of v1, /device:TPU:1, one launch (start us, length us, event | category | flops | bytes accessed | tf_op | source)
XLA Modules:
  0.0 297.8 jit_solution(4163561879144225295)
XLA Ops:
  0.6 4.0 %shard_map.188 = (f32[256,1]{1,0:T(8,128)}, f32[512,1]{1,0:T(8,128)}, bf16[64,16,512]{2,1,0:T(8,128)(2,1)}, bf16[512,256]{1,0:T(8,128)(2,1)}, bf16[64,16,512]{2,1,0:T(8,128)(2,1)}, /*index=5*/bf16[512,256]{1,0:T(8,128)(2,1)}) custom-call(s32[1]{0:T(128)} %bitcast.tp_ref, s32[2,256]{1,0:T(2,128)} %bitcast.24, f32[2,256]{1,0:T(2,128)} %bitcast.25, ...), custom_call_target="tpu_custom_call" | custom-call | tf_op jit(solution)/shard_map/pallas_call | solution.py:19
  4.6 41.4 %all_to_all.30.refs_0_ = bf16[64,16,512]{2,1,0:T(8,128)(2,1)} all-to-all(bf16[64,16,512]{2,1,0:T(8,128)(2,1)} %get-tuple-element.43), channel_id=1, replica_groups=mesh['sp'=64,'tp'=4] {'sp'}, dimensions={0} | all-to-all | bytes 2097152 | tf_op jit(solution)/shard_map/all_to_all | solution.py:295
  46.0 6.3 %all-to-all-start.3 = ((bf16[64,16,512]{2,1,0:T(8,128)(2,1)}), bf16[64,16,512]{2,1,0:T(8,128)(2,1)S(1)}, u32[]{:S(2)}, u32[]{:S(2)}) async-start(bf16[64,16,512]{2,1,0:T(8,128)(2,1)} %get-tuple-element.51), calls=%async_computation.3 | async-start | bytes 2097152 | tf_op jit(solution)/shard_map/all_to_all | solution.py:295
  52.3 3.3 %shard_map.190 = bf16[64,16,512]{2,1,0:T(8,128)(2,1)} custom-call(s32[1]{0:T(128)} %bitcast.tp_ref, bf16[512,256]{1,0:T(8,128)(2,1)} %get-tuple-element.48.pick_ref.pick1, f32[512,1]{1,0:T(8,128)} %get-tuple-element.49.weight_ref, f32[256,1]{1,0:T(8,128)} %get-tuple-element.50.rms_ref, bf16[256,2048]{1,0:T(8,128)(2,1)} %stream_ref.9, f32[1,2048]{1,0:T(1,128)} %bitcast.14, ...), custom_call_target="tpu_custom_call" | custom-call | tf_op jit(solution)/shard_map/pallas_call | solution.py:19
  55.6 24.9 %all-to-all-done.3.own.refs_8_ = bf16[64,16,512]{2,1,0:T(8,128)(2,1)S(1)} async-done(((bf16[64,16,512]{2,1,0:T(8,128)(2,1)}), bf16[64,16,512]{2,1,0:T(8,128)(2,1)S(1)}, u32[]{:S(2)}, u32[]{:S(2)}) %all-to-all-start.3) | async-done | bytes 1048608 | tf_op jit(solution)/shard_map/all_to_all | solution.py:295
  80.5 6.5 %all-to-all-start.2 = ((bf16[64,16,512]{2,1,0:T(8,128)(2,1)}), bf16[64,16,512]{2,1,0:T(8,128)(2,1)}, u32[]{:S(2)}, u32[]{:S(2)}) async-start(bf16[64,16,512]{2,1,0:T(8,128)(2,1)} %shard_map.190), calls=%async_computation.2 | async-start | bytes 2097152 | tf_op jit(solution)/shard_map/all_to_all | solution.py:295
  86.9 1.3 collective-permute-start.1
  88.2 1.5 collective-permute-start
  89.7 1.3 collective-permute-start.8
  91.2 21.6 %collective-permute-done.1.refs_2_ = bf16[64,16,512]{2,1,0:T(8,128)(2,1)S(1)} collective-permute-done((bf16[64,16,512]{2,1,0:T(8,128)(2,1)}, bf16[64,16,512]{2,1,0:T(8,128)(2,1)S(1)}, u32[]{:S(2)}, u32[]{:S(2)}) %collective-permute-start.1) | collective-permute-done | bytes 1048608 | tf_op jit(solution)/shard_map/ppermute | solution.py:325
  114.6 2.7 collective-permute-start.3
  117.2 17.6 %collective-permute-done.8.after.refs_9_ = bf16[64,16,512]{2,1,0:T(8,128)(2,1)S(1)} collective-permute-done((bf16[64,16,512]{2,1,0:T(8,128)(2,1)S(1)}, bf16[64,16,512]{2,1,0:T(8,128)(2,1)S(1)}, u32[]{:S(2)}, u32[]{:S(2)}) %collective-permute-start.8) | collective-permute-done | bytes 1048608 | tf_op jit(solution)/shard_map/ppermute | solution.py:325
  136.8 5.4 %shard_map.191 = (f32[512,256]{1,0:T(8,128)}, f32[512,256]{1,0:T(8,128)}, f32[512,256]{1,0:T(8,128)}) custom-call(s32[1]{0:T(128)} %bitcast.tp_ref, bf16[64,16,512]{2,1,0:T(8,128)(2,1)} %copy-done, bf16[64,16,512]{2,1,0:T(8,128)(2,1)} %copy-done.3, bf16[64,16,512]{2,1,0:T(8,128)(2,1)} %copy-done.4, bf16[1,2048,256]{2,1,0:T(8,128)(2,1)} %refs_4_.1, ...), custom_call_target="tpu_custom_call" | custom-call | flops 1342177280 | tf_op jit(solution)/shard_map/pallas_call | solution.py:19
  142.3 5.9 %shard_map.192 = (bf16[512,256]{1,0:T(8,128)(2,1)}, bf16[512,256]{1,0:T(8,128)(2,1)}, bf16[512,256]{1,0:T(8,128)(2,1)}, bf16[512,512]{1,0:T(8,128)(2,1)}, bf16[5...) custom-call(s32[1]{0:T(128)} %bitcast.tp_ref, ...), custom_call_target="tpu_custom_call" | custom-call | flops 2684354560 | tf_op jit(solution)/shard_map/pallas_call | solution.py:19
  148.2 2.5 collective-permute-start.12
  150.7 1.1 collective-permute-start.11
  152.2 8.6 %shard_map.189 = (bf16[512,256]{1,0:T(8,128)(2,1)}, bf16[512,256]{1,0:T(8,128)(2,1)}, bf16[512,256]{1,0:T(8,128)(2,1)}, bf16[512,512]{1,0:T(8,128)(2,1)}, bf16[5...) custom-call(s32[1]{0:T(128)} %bitcast.tp_ref, bf16[64,16,512]{2,1,0:T(8,128)(2,1)} %all_to_all.30.refs_0_, ...), custom_call_target="tpu_custom_call" | custom-call | flops 2684354560 | tf_op jit(solution)/shard_map/pallas_call | solution.py:19
  160.8 1.8 fusion.13
  162.6 2.4 collective-permute-start.6
  164.9 9.4 %collective-permute-done.11 = bf16[512,512]{1,0:T(8,128)(2,1)S(1)} collective-permute-done((bf16[512,512]{1,0:T(8,128)(2,1)}, bf16[512,512]{1,0:T(8,128)(2,1)S(1)}, u32[]{:S(2)}, u32[]{:S(2)}) %collective-permute-start.11) | collective-permute-done | bytes 524320 | tf_op jit(solution)/shard_map/ppermute | solution.py:325
  175.0 1.1 fusion.1
  176.1 13.8 %all-to-all-start.4 = ((bf16[64,8,512]{2,1,0:T(8,128)(2,1)}), bf16[64,8,512]{2,1,0:T(8,128)(2,1)S(1)}, u32[]{:S(2)}, u32[]{:S(2)}) async-start(bf16[64,8,512]{2,1,0:T(8,128)(2,1)} %fusion.1), calls=%async_computation.4 | async-start | bytes 1048576 | tf_op jit(solution)/shard_map/all_to_all | solution.py:295
  191.2 1.5 collective-permute-start.5
  192.7 11.4 %collective-permute-done.7 = bf16[512,512]{1,0:T(8,128)(2,1)S(1)} collective-permute-done((bf16[512,512]{1,0:T(8,128)(2,1)S(1)}, bf16[512,512]{1,0:T(8,128)(2,1)S(1)}, u32[]{:S(2)}, u32[]{:S(2)}) %collective-permute-start.7) | collective-permute-done | bytes 524320 | tf_op jit(solution)/shard_map/ppermute | solution.py:325
  204.1 1.2 collective-permute-done.5
  206.3 1.3 all-to-all-done.4.back1
  207.6 10.1 %all-to-all-start.1 = ((bf16[64,8,512]{2,1,0:T(8,128)(2,1)}), bf16[64,8,512]{2,1,0:T(8,128)(2,1)S(1)}, u32[]{:S(2)}, u32[]{:S(2)}) async-start(bf16[64,8,512]{2,1,0:T(8,128)(2,1)} %fusion), calls=%async_computation.1 | async-start | bytes 1048576 | tf_op jit(solution)/shard_map/all_to_all | solution.py:295
  217.8 3.5 %collective-permute-start.16 = (f32[2,256]{1,0:T(2,128)S(1)}, f32[2,256]{1,0:T(2,128)S(1)}, u32[]{:S(2)}, u32[]{:S(2)}) collective-permute-start(f32[2,256]{1,0:T(2,128)S(1)} %slice.57), channel_id=1, source_target_pairs={{0,4},{4,8},{8,12},{12,16},{16,20},{20,24},{24,28},{28,32},{32,36}... | collective-permute-start | bytes 6152 | tf_op jit(solution)/shard_map/ppermute | solution.py:291
  223.5 1.4 collective-permute-start.18
  225.0 10.5 %all-to-all-done.1.back0 = bf16[64,8,512]{2,1,0:T(8,128)(2,1)S(1)} async-done(((bf16[64,8,512]{2,1,0:T(8,128)(2,1)}), bf16[64,8,512]{2,1,0:T(8,128)(2,1)S(1)}, u32[]{:S(2)}, u32[]{:S(2)}) %all-to-all-start.1) | async-done | bytes 524320 | tf_op jit(solution)/shard_map/all_to_all | solution.py:295
  236.2 2.9 shard_map.193
  239.7 1.4 collective-permute-start.14
  241.8 2.1 collective-permute-done.14.s2
  243.8 1.4 collective-permute-done.15.s3
  245.9 3.5 %shard_map.194 = (bf16[256,512]{1,0:T(8,128)(2,1)}, f32[256,1]{1,0:T(8,128)}, bf16[16,2,32,256]{3,2,1,0:T(8,128)(2,1)}, bf16[16,2,32,256]{3,2,1,0:T(8,128)(2,1)}) custom-call(s32[1]{0:T(128)} %bitcast.tp_ref, s32[1]{0:T(128)} %bitcast.1.core_ref, bf16[256,512]{1,0:T(8,128)(2,1)} %get-tuple-element.59.token_ref, f32[1,256]{1,0:T(1,128)} %get-tuple-element.60.s0, ...), custom_call_target="tpu_custom_call" | custom-call | tf_op jit(solution)/shard_map/pallas_call | solution.py:19
  249.4 1.8 collective-permute-start.24
  251.2 1.7 collective-permute-done.24
  253.0 2.0 add_convert_fusion
  255.0 7.8 %all-to-all-start.5 = ((bf16[32,32,256]{2,1,0:T(8,128)(2,1)}), bf16[32,32,256]{2,1,0:T(8,128)(2,1)S(1)}, u32[]{:S(2)}, u32[]{:S(2)}) async-start(bf16[32,32,256]{2,1,0:T(8,128)(2,1)} %bitcast.10), calls=%async_computation.5 | async-start | bytes 1048576 | tf_op jit(solution)/shard_map/all_to_all | solution.py:295
  263.2 1.2 collective-permute-start.21
  265.2 9.9 %shard_map.196 = (f32[1,2048,256]{2,1,0:T(8,128)}, f32[1,2048,256]{2,1,0:T(8,128)}, f32[1,256,2048]{2,1,0:T(8,128)}) custom-call(s32[1]{0:T(128)} %bitcast.tp_ref, bf16[64,16,512]{2,1,0:T(8,128)(2,1)} %all_to_all.30.refs_0_, bf16[64,16,512]{2,1,0:T(8,128)(2,1)} %copy-done.17, bf16[64,16,512]{2,1,0:T(8,128)(2,1)} %copy-done.16, ...), custom_call_target="tpu_custom_call" | custom-call | flops 3221225472 | tf_op jit(solution)/shard_map/pallas_call | solution.py:19
  275.1 3.5 %collective-permute-done.22.t3 = bf16[256,512]{1,0:T(8,128)(2,1)S(1)} collective-permute-done((bf16[256,512]{1,0:T(8,128)(2,1)S(1)}, bf16[256,512]{1,0:T(8,128)(2,1)S(1)}, u32[]{:S(2)}, u32[]{:S(2)}) %collective-permute-start.22) | collective-permute-done | bytes 262176 | tf_op jit(solution)/shard_map/ppermute | solution.py:325
  279.3 3.8 %shard_map.195 = (bf16[256,256]{1,0:T(8,128)(2,1)}, f32[256,256]{1,0:T(8,128)}) custom-call(s32[1]{0:T(128)} %bitcast.tp_ref, bf16[256,512]{1,0:T(8,128)(2,1)} %get-tuple-element.93.g0, bf16[256,512]{1,0:T(8,128)(2,1)} %copy-done.13, bf16[256,512]{1,0:T(8,128)(2,1)} %copy-done.14, bf16[256,512]{1,0:T(8,128)(2,1)} %copy-done.15, ...), custom_call_target="tpu_custom_call" | custom-call | tf_op jit(solution)/shard_map/pallas_call | solution.py:19
  283.8 2.4 collective-permute-start.23
  287.1 1.5 collective-permute-done.23
  288.7 1.7 fusion.6
  290.5 1.9 collective-permute-start.25
  293.1 4.1 %collective-permute-done.25 = f32[32,256]{1,0:T(8,128)S(1)} collective-permute-done((f32[32,256]{1,0:T(8,128)S(1)}, f32[32,256]{1,0:T(8,128)S(1)}, u32[]{:S(2)}, u32[]{:S(2)}) %collective-permute-start.25) | collective-permute-done | bytes 32800 | tf_op jit(solution)/shard_map/ppermute | solution.py:451
  (95 shorter events, 16.9 us)
Async XLA Ops:
  46.0 34.4 %all-to-all-start.3 = ((bf16[64,16,512]{2,1,0:T(8,128)(2,1)}), bf16[64,16,512]{2,1,0:T(8,128)(2,1)S(1)}, u32[]{:S(2)}, u32[]{:S(2)}) async-start(bf16[64,16,512]{2,1,0:T(8,128)(2,1)} %get-tuple-element.51), calls=%async_computation.3 | async-start | bytes 2097152 | tf_op jit(solution)/shard_map/all_to_all | solution.py:295
  80.5 54.6 %copy-start = (bf16[64,16,512]{2,1,0:T(8,128)(2,1)}, bf16[64,16,512]{2,1,0:T(8,128)(2,1)S(1)}, u32[]{:S(2)}) copy-start(bf16[64,16,512]{2,1,0:T(8,128)(2,1)S(1)} %all-to-all-done.3.own.refs_8_) | copy-start | bytes 3145732
  80.5 61.8 %all-to-all-start.2 = ((bf16[64,16,512]{2,1,0:T(8,128)(2,1)}), bf16[64,16,512]{2,1,0:T(8,128)(2,1)}, u32[]{:S(2)}, u32[]{:S(2)}) async-start(bf16[64,16,512]{2,1,0:T(8,128)(2,1)} %shard_map.190), calls=%async_computation.2 | async-start | bytes 2097152 | tf_op jit(solution)/shard_map/all_to_all | solution.py:295
  86.9 25.8 %collective-permute-start.1 = (bf16[64,16,512]{2,1,0:T(8,128)(2,1)}, bf16[64,16,512]{2,1,0:T(8,128)(2,1)S(1)}, u32[]{:S(2)}, u32[]{:S(2)}) collective-permute-start(bf16[64,16,512]{2,1,0:T(8,128)(2,1)} %all_to_all.30.refs_0_), channel_id=1, source_target_pairs={{0,1},{1,2},{2,3},{3,0},{4,5},{5,6},{6,7},{7,4},{8,9},{9,10},{10,1... | collective-permute-start | bytes 3145736 | tf_op jit(solution)/shard_map/ppermute | solution.py:325
  88.2 25.4 %collective-permute-start = (bf16[64,16,512]{2,1,0:T(8,128)(2,1)}, bf16[64,16,512]{2,1,0:T(8,128)(2,1)S(1)}, u32[]{:S(2)}, u32[]{:S(2)}) collective-permute-start(bf16[64,16,512]{2,1,0:T(8,128)(2,1)} %all_to_all.30.refs_0_), channel_id=1, source_target_pairs={{0,3},{1,0},{2,1},{3,2},{4,7},{5,4},{6,5},{7,6},{8,11},{9,8},{10,9... | collective-permute-start | bytes 3145736 | tf_op jit(solution)/shard_map/ppermute | solution.py:325
  89.7 45.1 %collective-permute-start.8 = (bf16[64,16,512]{2,1,0:T(8,128)(2,1)S(1)}, bf16[64,16,512]{2,1,0:T(8,128)(2,1)S(1)}, u32[]{:S(2)}, u32[]{:S(2)}) collective-permute-start(bf16[64,16,512]{2,1,0:T(8,128)(2,1)S(1)} %all-to-all-done.3.own.refs_8_), channel_id=1, source_target_pairs={{0,3},{1,0},{2,1},{3,2},{4,7},{5,4},{6,5},{7,6},{8,11},{9,8},{10,9... | collective-permute-start | bytes 3145736 | tf_op jit(solution)/shard_map/ppermute | solution.py:325
  91.0 44.1 %collective-permute-start.9 = (bf16[64,16,512]{2,1,0:T(8,128)(2,1)S(1)}, bf16[64,16,512]{2,1,0:T(8,128)(2,1)S(1)}, u32[]{:S(2)}, u32[]{:S(2)}) collective-permute-start(bf16[64,16,512]{2,1,0:T(8,128)(2,1)S(1)} %all-to-all-done.3.own.refs_8_), channel_id=1, source_target_pairs={{0,1},{1,2},{2,3},{3,0},{4,5},{5,6},{6,7},{7,4},{8,9},{9,10},{10,1... | collective-permute-start | bytes 3145736 | tf_op jit(solution)/shard_map/ppermute | solution.py:325
  112.7 22.1 %copy-start.16 = (bf16[64,16,512]{2,1,0:T(8,128)(2,1)}, bf16[64,16,512]{2,1,0:T(8,128)(2,1)S(1)}, u32[]{:S(2)}) copy-start(bf16[64,16,512]{2,1,0:T(8,128)(2,1)S(1)} %collective-permute-done.1.refs_2_) | copy-start | bytes 3145732
  113.6 38.5 %collective-permute-start.2 = (bf16[64,8,512]{2,1,0:T(8,128)(2,1)}, bf16[64,8,512]{2,1,0:T(8,128)(2,1)}, u32[]{:S(2)}, u32[]{:S(2)}) collective-permute-start(bf16[64,8,512]{2,1,0:T(8,128)(2,1)} %slice.55), channel_id=1, source_target_pairs={{0,1},{1,2},{2,3},{3,0},{4,5},{5,6},{6,7},{7,4},{8,9},{9,10},{10,1... | collective-permute-start | bytes 1572872 | tf_op jit(solution)/shard_map/ppermute | solution.py:325
  113.7 21.2 %copy-start.17 = (bf16[64,16,512]{2,1,0:T(8,128)(2,1)}, bf16[64,16,512]{2,1,0:T(8,128)(2,1)S(1)}, u32[]{:S(2)}) copy-start(bf16[64,16,512]{2,1,0:T(8,128)(2,1)S(1)} %collective-permute-done.refs_1_) | copy-start | bytes 3145732
  114.6 37.6 %collective-permute-start.3 = (bf16[64,8,512]{2,1,0:T(8,128)(2,1)}, bf16[64,8,512]{2,1,0:T(8,128)(2,1)}, u32[]{:S(2)}, u32[]{:S(2)}) collective-permute-start(bf16[64,8,512]{2,1,0:T(8,128)(2,1)} %slice.56), channel_id=1, source_target_pairs={{0,3},{1,0},{2,1},{3,2},{4,7},{5,4},{6,5},{7,6},{8,11},{9,8},{10,9... | collective-permute-start | bytes 1572872 | tf_op jit(solution)/shard_map/ppermute | solution.py:325
  148.2 16.7 %collective-permute-start.12 = (bf16[512,512]{1,0:T(8,128)(2,1)}, bf16[512,512]{1,0:T(8,128)(2,1)S(1)}, u32[]{:S(2)}, u32[]{:S(2)}) collective-permute-start(bf16[512,512]{1,0:T(8,128)(2,1)} %get-tuple-element.58), channel_id=1, source_target_pairs={{0,2},{1,3},{2,0},{3,1},{4,6},{5,7},{6,4},{7,5},{8,10},{9,11},{10,... | collective-permute-start | bytes 1572872 | tf_op jit(solution)/shard_map/ppermute | solution.py:325
  150.7 23.7 %collective-permute-start.11 = (bf16[512,512]{1,0:T(8,128)(2,1)}, bf16[512,512]{1,0:T(8,128)(2,1)S(1)}, u32[]{:S(2)}, u32[]{:S(2)}) collective-permute-start(bf16[512,512]{1,0:T(8,128)(2,1)} %get-tuple-element.57), channel_id=1, source_target_pairs={{0,3},{1,0},{2,1},{3,2},{4,7},{5,4},{6,5},{7,6},{8,11},{9,8},{10,9... | collective-permute-start | bytes 1572872 | tf_op jit(solution)/shard_map/ppermute | solution.py:325
  151.8 23.2 %copy-start.5 = (bf16[512,512]{1,0:T(8,128)(2,1)S(1)}, bf16[512,512]{1,0:T(8,128)(2,1)}, u32[]{:S(2)}) copy-start(bf16[512,512]{1,0:T(8,128)(2,1)} %get-tuple-element.55) | copy-start | bytes 1572868
  151.8 23.2 %collective-permute-start.10 = (bf16[512,512]{1,0:T(8,128)(2,1)}, bf16[512,512]{1,0:T(8,128)(2,1)S(1)}, u32[]{:S(2)}, u32[]{:S(2)}) collective-permute-start(bf16[512,512]{1,0:T(8,128)(2,1)} %get-tuple-element.56), channel_id=1, source_target_pairs={{0,1},{1,2},{2,3},{3,0},{4,5},{5,6},{6,7},{7,4},{8,9},{9,10},{10,1... | collective-permute-start | bytes 1572872 | tf_op jit(solution)/shard_map/ppermute | solution.py:325
  162.6 27.3 %copy-start.7 = (bf16[512,512]{1,0:T(8,128)(2,1)S(1)}, bf16[512,512]{1,0:T(8,128)(2,1)}, u32[]{:S(2)}) copy-start(bf16[512,512]{1,0:T(8,128)(2,1)} %get-tuple-element.47) | copy-start | bytes 1572868
  162.6 27.3 %collective-permute-start.6 = (bf16[256,512]{1,0:T(8,128)(2,1)}, bf16[256,512]{1,0:T(8,128)(2,1)}, u32[]{:S(2)}, u32[]{:S(2)}) collective-permute-start(bf16[256,512]{1,0:T(8,128)(2,1)} %get-tuple-element.81), channel_id=1, source_target_pairs={{0,3},{1,0},{2,1},{3,2},{4,7},{5,4},{6,5},{7,6},{8,11},{9,8},{10,9... | collective-permute-start | bytes 786440 | tf_op jit(solution)/shard_map/ppermute | solution.py:325
  164.9 26.1 %collective-permute-start.4 = (bf16[256,512]{1,0:T(8,128)(2,1)}, bf16[256,512]{1,0:T(8,128)(2,1)S(1)}, u32[]{:S(2)}, u32[]{:S(2)}) collective-permute-start(bf16[256,512]{1,0:T(8,128)(2,1)} %get-tuple-element.80), channel_id=1, source_target_pairs={{0,1},{1,2},{2,3},{3,0},{4,5},{5,6},{6,7},{7,4},{8,9},{9,10},{10,1... | collective-permute-start | bytes 786440 | tf_op jit(solution)/shard_map/ppermute | solution.py:325
  175.0 16.0 %copy-start.6 = (bf16[512,512]{1,0:T(8,128)(2,1)S(1)}, bf16[512,512]{1,0:T(8,128)(2,1)}, u32[]{:S(2)}) copy-start(bf16[512,512]{1,0:T(8,128)(2,1)} %get-tuple-element.45) | copy-start | bytes 1572868
  176.1 29.2 %copy-start.11 = (bf16[512,512]{1,0:T(8,128)(2,1)S(1)}, bf16[512,512]{1,0:T(8,128)(2,1)}, u32[]{:S(2)}) copy-start(bf16[512,512]{1,0:T(8,128)(2,1)} %get-tuple-element.44) | copy-start | bytes 1572868
  176.1 31.5 %all-to-all-start.4 = ((bf16[64,8,512]{2,1,0:T(8,128)(2,1)}), bf16[64,8,512]{2,1,0:T(8,128)(2,1)S(1)}, u32[]{:S(2)}, u32[]{:S(2)}) async-start(bf16[64,8,512]{2,1,0:T(8,128)(2,1)} %fusion.1), calls=%async_computation.4 | async-start | bytes 1048576 | tf_op jit(solution)/shard_map/all_to_all | solution.py:295
  191.0 13.1 %collective-permute-start.7 = (bf16[512,512]{1,0:T(8,128)(2,1)S(1)}, bf16[512,512]{1,0:T(8,128)(2,1)S(1)}, u32[]{:S(2)}, u32[]{:S(2)}) collective-permute-start(bf16[512,512]{1,0:T(8,128)(2,1)S(1)} %add_convert_fusion.3), channel_id=1, source_target_pairs={{0,3},{1,0},{2,1},{3,2},{4,7},{5,4},{6,5},{7,6},{8,11},{9,8},{10,9... | collective-permute-start | bytes 1572872 | tf_op jit(solution)/shard_map/ppermute | solution.py:325
  191.1 26.7 %copy-start.9 = (bf16[256,256]{1,0:T(8,128)(2,1)S(1)}, bf16[256,256]{1,0:T(8,128)(2,1)}, u32[]{:S(2)}) copy-start(bf16[256,256]{1,0:T(8,128)(2,1)} %param.17) | copy-start | bytes 393220
  191.1 26.7 %copy-start.12 = (bf16[256,256]{1,0:T(8,128)(2,1)S(1)}, bf16[256,256]{1,0:T(8,128)(2,1)}, u32[]{:S(2)}) copy-start(bf16[256,256]{1,0:T(8,128)(2,1)} %param.18) | copy-start | bytes 393220
  191.2 30.2 %copy-start.22 = (f32[3,256]{1,0:T(4,128)S(1)}, f32[3,256]{1,0:T(4,128)}, u32[]{:S(2)}) copy-start(f32[3,256]{1,0:T(4,128)} %param.19) | copy-start | bytes 9220
  191.2 30.9 %copy-start.8 = (bf16[256,256]{1,0:T(8,128)(2,1)S(1)}, bf16[256,256]{1,0:T(8,128)(2,1)}, u32[]{:S(2)}) copy-start(bf16[256,256]{1,0:T(8,128)(2,1)} %gate_ref.3) | copy-start | bytes 393220
  191.2 14.1 %collective-permute-start.5 = (bf16[512,512]{1,0:T(8,128)(2,1)S(1)}, bf16[512,512]{1,0:T(8,128)(2,1)S(1)}, u32[]{:S(2)}, u32[]{:S(2)}) collective-permute-start(bf16[512,512]{1,0:T(8,128)(2,1)S(1)} %add_convert_fusion.4), channel_id=1, source_target_pairs={{0,1},{1,2},{2,3},{3,0},{4,5},{5,6},{6,7},{7,4},{8,9},{9,10},{10,1... | collective-permute-start | bytes 1572872 | tf_op jit(solution)/shard_map/ppermute | solution.py:325
  207.6 27.9 %copy-start.1 = (bf16[64,8,512]{2,1,0:T(8,128)(2,1)}, bf16[64,8,512]{2,1,0:T(8,128)(2,1)S(1)}, u32[]{:S(2)}) copy-start(bf16[64,8,512]{2,1,0:T(8,128)(2,1)S(1)} %all-to-all-done.4.back1) | copy-start | bytes 1572868
  207.6 27.8 %all-to-all-start.1 = ((bf16[64,8,512]{2,1,0:T(8,128)(2,1)}), bf16[64,8,512]{2,1,0:T(8,128)(2,1)S(1)}, u32[]{:S(2)}, u32[]{:S(2)}) async-start(bf16[64,8,512]{2,1,0:T(8,128)(2,1)} %fusion), calls=%async_computation.1 | async-start | bytes 1048576 | tf_op jit(solution)/shard_map/all_to_all | solution.py:295
  217.8 4.3 %collective-permute-start.16 = (f32[2,256]{1,0:T(2,128)S(1)}, f32[2,256]{1,0:T(2,128)S(1)}, u32[]{:S(2)}, u32[]{:S(2)}) collective-permute-start(f32[2,256]{1,0:T(2,128)S(1)} %slice.57), channel_id=1, source_target_pairs={{0,4},{4,8},{8,12},{12,16},{16,20},{20,24},{24,28},{28,32},{32,36}... | collective-permute-start | bytes 6152 | tf_op jit(solution)/shard_map/ppermute | solution.py:291
  222.9 22.4 %copy-start.10 = (bf16[256,256]{1,0:T(8,128)(2,1)}, bf16[256,256]{1,0:T(8,128)(2,1)S(1)}, u32[]{:S(2)}) copy-start(bf16[256,256]{1,0:T(8,128)(2,1)S(1)} %get-tuple-element.78.m0) | copy-start | bytes 393220
  222.9 18.2 %collective-permute-start.17 = (bf16[256,256]{1,0:T(8,128)(2,1)S(1)}, bf16[256,256]{1,0:T(8,128)(2,1)S(1)}, u32[]{:S(2)}, u32[]{:S(2)}) collective-permute-start(bf16[256,256]{1,0:T(8,128)(2,1)S(1)} %get-tuple-element.78.m0), channel_id=1, source_target_pairs={{0,3},{1,0},{2,1},{3,2},{4,7},{5,4},{6,5},{7,6},{8,11},{9,8},{10,9... | collective-permute-start | bytes 393224 | tf_op jit(solution)/shard_map/ppermute | solution.py:325
  223.5 17.7 %collective-permute-start.18 = (bf16[256,256]{1,0:T(8,128)(2,1)S(1)}, bf16[256,256]{1,0:T(8,128)(2,1)S(1)}, u32[]{:S(2)}, u32[]{:S(2)}) collective-permute-start(bf16[256,256]{1,0:T(8,128)(2,1)S(1)} %get-tuple-element.78.m0), channel_id=1, source_target_pairs={{0,2},{1,3},{2,0},{3,1},{4,6},{5,7},{6,4},{7,5},{8,10},{9,11},{10,... | collective-permute-start | bytes 393224 | tf_op jit(solution)/shard_map/ppermute | solution.py:325
  224.9 16.3 %collective-permute-start.19 = (bf16[256,256]{1,0:T(8,128)(2,1)S(1)}, bf16[256,256]{1,0:T(8,128)(2,1)S(1)}, u32[]{:S(2)}, u32[]{:S(2)}) collective-permute-start(bf16[256,256]{1,0:T(8,128)(2,1)S(1)} %get-tuple-element.78.m0), channel_id=1, source_target_pairs={{0,1},{1,2},{2,3},{3,0},{4,5},{5,6},{6,7},{7,4},{8,9},{9,10},{10,1... | collective-permute-start | bytes 393224 | tf_op jit(solution)/shard_map/ppermute | solution.py:325
  239.2 2.6 collective-permute-start.13
  239.7 4.1 %collective-permute-start.14 = (f32[1,256]{1,0:T(1,128)}, f32[1,256]{1,0:T(1,128)S(1)}, u32[]{:S(2)}, u32[]{:S(2)}) collective-permute-start(f32[1,256]{1,0:T(1,128)} %get-tuple-element.60.s0), channel_id=1, source_target_pairs={{0,2},{1,3},{2,0},{3,1},{4,6},{5,7},{6,4},{7,5},{8,10},{9,11},{10,... | collective-permute-start | bytes 3080 | tf_op jit(solution)/shard_map/ppermute | solution.py:325
  241.2 4.1 %copy-start.19 = (bf16[256,256]{1,0:T(8,128)(2,1)}, bf16[256,256]{1,0:T(8,128)(2,1)S(1)}, u32[]{:S(2)}) copy-start(bf16[256,256]{1,0:T(8,128)(2,1)S(1)} %collective-permute-done.17.m1) | copy-start | bytes 393220
  241.2 4.1 %collective-permute-start.15 = (f32[1,256]{1,0:T(1,128)}, f32[1,256]{1,0:T(1,128)S(1)}, u32[]{:S(2)}, u32[]{:S(2)}) collective-permute-start(f32[1,256]{1,0:T(1,128)} %get-tuple-element.60.s0), channel_id=1, source_target_pairs={{0,1},{1,2},{2,3},{3,0},{4,5},{5,6},{6,7},{7,4},{8,9},{9,10},{10,1... | collective-permute-start | bytes 3080 | tf_op jit(solution)/shard_map/ppermute | solution.py:325
  241.2 4.1 %copy-start.20 = (bf16[256,256]{1,0:T(8,128)(2,1)}, bf16[256,256]{1,0:T(8,128)(2,1)S(1)}, u32[]{:S(2)}) copy-start(bf16[256,256]{1,0:T(8,128)(2,1)S(1)} %collective-permute-done.18.m2) | copy-start | bytes 393220
  241.2 4.1 %copy-start.21 = (bf16[256,256]{1,0:T(8,128)(2,1)}, bf16[256,256]{1,0:T(8,128)(2,1)S(1)}, u32[]{:S(2)}) copy-start(bf16[256,256]{1,0:T(8,128)(2,1)S(1)} %collective-permute-done.19.m3) | copy-start | bytes 393220
  245.8 16.9 %copy-start.18 = (bf16[256,512]{1,0:T(8,128)(2,1)S(1)}, bf16[256,512]{1,0:T(8,128)(2,1)}, u32[]{:S(2)}) copy-start(bf16[256,512]{1,0:T(8,128)(2,1)} %get-tuple-element.59.token_ref) | copy-start | bytes 786436
  249.4 3.6 %collective-permute-start.24 = (bf16[16,2,32,256]{3,2,1,0:T(8,128)(2,1)}, bf16[16,2,32,256]{3,2,1,0:T(8,128)(2,1)S(1)}, u32[]{:S(2)}, u32[]{:S(2)}) collective-permute-start(bf16[16,2,32,256]{3,2,1,0:T(8,128)(2,1)} %get-tuple-element.66), channel_id=1, source_target_pairs={{0,4},{4,0},{8,12},{12,8},{16,20},{20,16},{24,28},{28,24},{32,36},... | collective-permute-start | bytes 1572872 | tf_op jit(solution)/shard_map/ppermute | solution.py:440
  255.0 35.4 %all-to-all-start.5 = ((bf16[32,32,256]{2,1,0:T(8,128)(2,1)}), bf16[32,32,256]{2,1,0:T(8,128)(2,1)S(1)}, u32[]{:S(2)}, u32[]{:S(2)}) async-start(bf16[32,32,256]{2,1,0:T(8,128)(2,1)} %bitcast.10), calls=%async_computation.5 | async-start | bytes 1048576 | tf_op jit(solution)/shard_map/all_to_all | solution.py:295
  262.8 12.3 %collective-permute-start.20 = (bf16[256,512]{1,0:T(8,128)(2,1)S(1)}, bf16[256,512]{1,0:T(8,128)(2,1)S(1)}, u32[]{:S(2)}, u32[]{:S(2)}) collective-permute-start(bf16[256,512]{1,0:T(8,128)(2,1)S(1)} %copy-done.18), channel_id=1, source_target_pairs={{0,3},{1,0},{2,1},{3,2},{4,7},{5,4},{6,5},{7,6},{8,11},{9,8},{10,9... | collective-permute-start | bytes 786440 | tf_op jit(solution)/shard_map/ppermute | solution.py:325
  263.2 11.9 %collective-permute-start.21 = (bf16[256,512]{1,0:T(8,128)(2,1)S(1)}, bf16[256,512]{1,0:T(8,128)(2,1)S(1)}, u32[]{:S(2)}, u32[]{:S(2)}) collective-permute-start(bf16[256,512]{1,0:T(8,128)(2,1)S(1)} %copy-done.18), channel_id=1, source_target_pairs={{0,2},{1,3},{2,0},{3,1},{4,6},{5,7},{6,4},{7,5},{8,10},{9,11},{10,... | collective-permute-start | bytes 786440 | tf_op jit(solution)/shard_map/ppermute | solution.py:325
  264.4 14.2 %collective-permute-start.22 = (bf16[256,512]{1,0:T(8,128)(2,1)S(1)}, bf16[256,512]{1,0:T(8,128)(2,1)S(1)}, u32[]{:S(2)}, u32[]{:S(2)}) collective-permute-start(bf16[256,512]{1,0:T(8,128)(2,1)S(1)} %copy-done.18), channel_id=1, source_target_pairs={{0,1},{1,2},{2,3},{3,0},{4,5},{5,6},{6,7},{7,4},{8,9},{9,10},{10,1... | collective-permute-start | bytes 786440 | tf_op jit(solution)/shard_map/ppermute | solution.py:325
  283.8 4.9 %collective-permute-start.23 = (f32[2,256]{1,0:T(2,128)S(1)}, f32[2,256]{1,0:T(2,128)S(1)}, u32[]{:S(2)}, u32[]{:S(2)}) collective-permute-start(f32[2,256]{1,0:T(2,128)S(1)} %slice.52), channel_id=1, source_target_pairs={{4,0},{8,4},{12,8},{16,12},{20,16},{24,20},{28,24},{32,28},{36,32}... | collective-permute-start | bytes 6152 | tf_op jit(solution)/shard_map/ppermute | solution.py:291
  290.5 6.7 %collective-permute-start.25 = (f32[32,256]{1,0:T(8,128)S(1)}, f32[32,256]{1,0:T(8,128)S(1)}, u32[]{:S(2)}, u32[]{:S(2)}) collective-permute-start(f32[32,256]{1,0:T(8,128)S(1)} %convert_reduce_fusion), channel_id=1, source_target_pairs={{0,0},{1,64},{2,128},{3,192},{4,1},{5,65},{6,129},{7,193},{8,2},{9... | collective-permute-start | bytes 98312 | tf_op jit(solution)/shard_map/ppermute | solution.py:451
  (9 other events, 16.0 us)
